TPU v7x, 256 devices: a whole 4x4x8 slice. The times are simulated.
256 devices in a mesh: fs: 64 (over z, x, core), tp: 4 (over y).
Axes of the slice: x: 4, y: 4, z: 8, core: 2. Of those that a mesh axis runs over, the one named last changes fastest.
Arguments:
- tokens: bfloat16 [768, 4, 2048], P(None, 'tp'), may hold values from -6 to 6
- norm_gain: float32 [2048], P('fs'), may hold values from 0.1 to 1.9
- gate_weight: float32 [8, 2048, 4096], P(None, 'fs', 'tp'), may hold values from -0.125 to 0.125
- up_weight: float32 [8, 2048, 4096], P(None, 'fs', 'tp'), may hold values from -0.125 to 0.125
- down_weight: float32 [8, 2048, 4096], P(None, 'fs', 'tp'), may hold values from -0.09375 to 0.09375
- expert_ids: int32 [768, 4, 2], P(None, 'tp'), may hold values from 0 to 7, all different within a row
- expert_mix: float32 [768, 4, 2], P(None, 'tp'), may hold values from 0.2 to 1
Outputs:
- gate_serve: bfloat16 [8, 2048, 4096], P(None, None, 'fs')
- up_serve: bfloat16 [8, 2048, 4096], P(None, None, 'fs')
- down_serve: bfloat16 [8, 2048, 4096], P(None, None, 'fs')
- mixed: bfloat16 [768, 4, 2048], P('fs', 'tp')
Inputs may be any that keep to these rules, and one draw needn't show every extreme that they name: `expert_ids`: each token names two different experts.
All inputs are finite; a program needn't handle non-finite values.
Results may differ from a plain program's by a relative error of at most 0.0082.
Values may be sent and summed in bfloat16 or wider, within the bound.
No kernel may reach another device: no remote copies, remote signals or barrier semaphores. Data moves between devices by JAX's collectives and lax.ppermute only.
A program may use at most 64 MiB of HBM per device.

v0:
```python
import jax
import jax.numpy as jnp
from jax import lax
from jax.experimental import pallas as pl
from jax.experimental.pallas import tpu as pltpu
from jax.sharding import Mesh
from jax.sharding import PartitionSpec as P

FS = ("fs_0", "fs_1", "fs_2")
VMEM_LIMIT = pltpu.CompilerParams(vmem_limit_bytes=16 << 20)

norm_eps = 1e-05
D_WIDTHS = (1024, 1024)
RELAYED = {"g": 1, "u": -1}

VMEM = pl.BlockSpec(memory_space=pltpu.VMEM)
SMEM = pl.BlockSpec(memory_space=pltpu.SMEM)


def shifted(array, axis, by):
    n = lax.axis_size(axis)
    return lax.ppermute(array, axis, [(i, (i + by) % n) for i in range(n)])


def prepare(tp_index, gain, weights, scaled):
    experts, rows, columns = weights[0].shape
    n_tp = lax.axis_size("tp")
    per = experts // n_tp
    n = len(weights)

    def body(tp_ref, gain_ref, *refs):
        outs = refs[n:]
        low = lax.broadcasted_iota(jnp.int32, (rows, 128), 1) < 64
        spread = jnp.broadcast_to(gain_ref[...], (rows, rows))
        across = lax.broadcasted_iota(jnp.int32, (rows, rows), 1)
        down = lax.broadcasted_iota(jnp.int32, (rows, rows), 0)
        scale = jnp.sum(jnp.where(across == down, spread, 0.0), axis=1, keepdims=True)
        scale = jnp.broadcast_to(scale, (rows, 128))
        for s in range(n_tp):
            first = lax.rem(tp_ref[0] + s, n_tp) * per

            def one(pair, _, s=s, first=first):
                at = pl.ds(pl.multiple_of(pair * 128, 128), 128)
                for m in range(n):
                    a, b = refs[m][first, :, at], refs[m][first + 1, :, at]
                    if scaled[m]:
                        a, b = a * scale, b * scale
                    even = jnp.where(low, a, pltpu.roll(b, 64, 1))
                    odd = jnp.where(low, pltpu.roll(a, 64, 1), b)
                    outs[s][2 * pair, m] = even.astype(jnp.bfloat16)
                    outs[s][2 * pair + 1, m] = odd.astype(jnp.bfloat16)
                return 0

            lax.fori_loop(0, columns // 128, one, 0, unroll=2)

    return pl.pallas_call(
        body,
        out_shape=[jax.ShapeDtypeStruct((columns // 64, n, rows, 128), jnp.bfloat16)] * n_tp,
        in_specs=[SMEM] + [VMEM] * (n + 1),
        out_specs=[VMEM] * n_tp,
        compiler_params=VMEM_LIMIT,
        name="prepare",
    )(tp_index, gain[None, :], *weights)


def placed(slots, blocks):
    n = len(blocks)

    def body(slot_ref, *refs):
        for i in range(n):
            refs[n][slot_ref[i]] = refs[i][...]

    return pl.pallas_call(
        body,
        out_shape=jax.ShapeDtypeStruct((n,) + blocks[0].shape, blocks[0].dtype),
        in_specs=[SMEM] + [VMEM] * n,
        out_specs=VMEM,
        compiler_params=VMEM_LIMIT,
        name="placed",
    )(slots, *blocks)


def fill(slot_ref, refs, all_ref):
    for i, ref in enumerate(refs):
        at = pl.multiple_of(slot_ref[i] * 64, 64)
        all_ref[pl.ds(at, ref.shape[0]), :] = ref[...]


def acted(slots, normed, blocks, gate_act=None, gates=None):
    tokens, width = normed.shape
    n = len(blocks)
    units = 512
    step = tokens // 2
    last = gate_act is not None

    def body(slot_ref, n_ref, *refs):
        all_ref, out_ref = refs[-2:]
        fill(slot_ref, refs[:n], all_ref)
        low = lax.broadcasted_iota(jnp.int32, (step, 128), 1) < 64

        def one(i, _):
            rows = pl.ds(pl.multiple_of(i * step, step), step)
            for at in range(0, units, 256):
                act = lax.dot_general(
                    n_ref[rows, :],
                    all_ref[pl.ds(at, 256), :],
                    (((1,), (1,)), ((), ())),
                    preferred_element_type=jnp.float32,
                )
                if not last:
                    out_ref[rows, pl.ds(at, 256)] = act
                    continue
                for half in range(2):
                    cols = pl.ds(at + half * 128, 128)
                    e = (at + half * 128) // 64
                    mix = jnp.where(
                        low, refs[n + 1][rows, e : e + 1], refs[n + 1][rows, e + 1 : e + 2]
                    )
                    up = act[:, half * 128 : (half + 1) * 128]
                    hidden = jax.nn.silu(refs[n][rows, cols]) * up * mix
                    out_ref[rows, cols] = hidden.astype(jnp.bfloat16)
            return 0

        lax.fori_loop(0, 2, one, 0)

    args = [slots, normed, *blocks] + ([gate_act, gates] if last else [])
    return pl.pallas_call(
        body,
        out_shape=[
            jax.ShapeDtypeStruct((units, width), jnp.bfloat16),
            jax.ShapeDtypeStruct((tokens, units), jnp.bfloat16 if last else jnp.float32),
        ],
        in_specs=[SMEM] + [VMEM] * (len(args) - 1),
        out_specs=[VMEM] * 2,
        compiler_params=pltpu.CompilerParams(vmem_limit_bytes=24 << 20),
        name="acted",
    )(*args)


def turned(block, widths):
    _, n, rows, lanes = block.shape
    step = 256 // rows
    outs = [(m, w) for m in range(n) for w in widths]

    def body(x_ref, *refs):
        for k, (m, width) in enumerate(outs):
            start = sum(w for p, w in outs[:k] if p == m) // rows

            def one(i, _, out=refs[k], m=m, start=start):
                t = x_ref[pl.ds(start + i * step, step), m].reshape(256, lanes).T
                out[:, pl.ds(pl.multiple_of(i * 256, 256), 256)] = t
                return 0

            lax.fori_loop(0, width // 256, one, 0)

    return pl.pallas_call(
        body,
        out_shape=[jax.ShapeDtypeStruct((lanes, w), block.dtype) for _, w in outs],
        in_specs=[VMEM],
        out_specs=[VMEM] * len(outs),
        compiler_params=VMEM_LIMIT,
        name="turned",
    )(block)


def gathered(name, own):
    n_tp = lax.axis_size("tp")
    tp = lax.axis_index("tp").astype(jnp.int32)

    def sent(block, by):
        return shifted(block, "tp", by)

    prev, after = sent(own, 1), sent(own, -1)
    slots = [2 * tp, 2 * ((tp - 1) % n_tp), 2 * ((tp + 1) % n_tp), 2 * ((tp + 2) % n_tp)]
    if name in RELAYED:
        far = [sent(*((prev, 1) if RELAYED[name] > 0 else (after, -1)))]
    else:
        far = [sent(own, 2)]
    return jnp.stack(slots), [own, prev, after] + far


def mixed_away(slots, hidden, blocks):
    tokens, units = hidden.shape
    half = tokens // 2
    wide = blocks[0].shape[1]
    n = len(blocks)

    def body(slot_ref, h_ref, *refs):
        all_ref, away_ref = refs[n:]
        fill(slot_ref, refs[:n], all_ref)

        def one(i, _):
            at = pl.ds(pl.multiple_of(i * 256, 256), 256)
            part = jnp.dot(h_ref[half:], all_ref[:, at], preferred_element_type=jnp.float32)
            away_ref[:, at] = part.astype(jnp.bfloat16)
            return 0

        lax.fori_loop(0, wide // 256, one, 0)

    return pl.pallas_call(
        body,
        out_shape=[
            jax.ShapeDtypeStruct((units, wide), jnp.bfloat16),
            jax.ShapeDtypeStruct((half, wide), jnp.bfloat16),
        ],
        in_specs=[SMEM] + [VMEM] * (n + 1),
        out_specs=[VMEM] * 2,
        compiler_params=VMEM_LIMIT,
        name="mixed_away",
    )(slots, hidden, *blocks)


def mixed_here(hidden, down, arrived, n_x):
    half, wide = arrived.shape
    rows = half // n_x

    def body(h_ref, d_ref, r_ref, *outs):
        def one(i, _):
            at = pl.ds(pl.multiple_of(i * 256, 256), 256)
            part = jnp.dot(h_ref[:half], d_ref[:, at], preferred_element_type=jnp.float32)
            part = part + r_ref[:, at].astype(jnp.float32)
            for x in range(n_x):
                outs[x][:, at] = part[x * rows : (x + 1) * rows].astype(outs[x].dtype)
            return 0

        lax.fori_loop(0, wide // 256, one, 0)

    return pl.pallas_call(
        body,
        out_shape=[
            jax.ShapeDtypeStruct((rows, wide), jnp.bfloat16 if x else jnp.float32)
            for x in range(n_x)
        ],
        in_specs=[VMEM] * 3,
        out_specs=[VMEM] * n_x,
        compiler_params=VMEM_LIMIT,
        name="mixed_here",
    )(hidden, down, arrived)


def folded(parts, n_z):
    widths = [p[0].shape[1] for p in parts]
    count = parts[0][0].shape[0]
    width = sum(widths)
    rows, half = count // n_z, width // 2
    flat = [a for p in parts for a in p]
    per = len(parts[0])

    def body(*refs):
        out, total = refs[-2:]
        start = 0
        for c, wide in enumerate(widths):
            part = refs[c * per][...]
            for i in range(1, per):
                part = part + refs[c * per + i][...].astype(jnp.float32)
            total[:, pl.ds(start, wide)] = part
            start += wide
        for z in range(n_z):
            at = pl.ds(z * rows, rows)
            piece = jnp.concatenate([total[at, :half], total[at, half:]], axis=0)
            out[z] = piece.astype(out.dtype)

    return pl.pallas_call(
        body,
        out_shape=jax.ShapeDtypeStruct((n_z, 2 * rows, half), jnp.bfloat16),
        in_specs=[VMEM] * len(flat),
        out_specs=VMEM,
        scratch_shapes=[pltpu.VMEM((count, width), jnp.float32)],
        compiler_params=VMEM_LIMIT,
        name="folded",
    )(*flat)


def finished(pieces):
    n_z, rows, half = pieces.shape

    def body(p_ref, out):
        total = p_ref[0].astype(jnp.float32)
        for z in range(1, n_z):
            total = total + p_ref[z].astype(jnp.float32)
        wide = jnp.concatenate([total[: rows // 2], total[rows // 2 :]], axis=1)
        out[...] = wide.astype(jnp.bfloat16)

    return pl.pallas_call(
        body,
        out_shape=jax.ShapeDtypeStruct((rows // 2, 2 * half), jnp.bfloat16),
        in_specs=[VMEM],
        out_specs=VMEM,
        compiler_params=VMEM_LIMIT,
        name="finished",
    )(pieces)


def local(tokens, norm_gain, gate_weight, up_weight, down_weight, expert_ids, expert_mix):
    tp = lax.axis_index("tp").astype(jnp.int32)
    tp_index = tp.reshape(1)
    n_tp = lax.axis_size("tp")
    column_slots = jnp.stack([(tp - s) % n_tp for s in range(n_tp)])

    def handed(weights, scaled):
        blocks = prepare(tp_index, norm_gain, weights, scaled)
        arrived = [blocks[0]]
        for s in range(1, n_tp):
            arrived.append(shifted(blocks[s], "tp", s))
        columns = placed(column_slots, arrived)
        columns = columns.reshape((-1,) + columns.shape[2:])
        return lax.all_to_all(columns, FS, split_axis=0, concat_axis=0, tiled=True)

    block_a = handed((gate_weight, up_weight), (True, True))
    block_d = handed((down_weight,), (False,))
    gate_own, up_own = turned(block_a, (tokens.shape[2],))
    down_own = turned(block_d, D_WIDTHS)
    gate_pieces = gathered("g", gate_own)
    up_pieces = gathered("u", up_own)
    down_pieces = [gathered(f"d{c}", own) for c, own in enumerate(down_own)]

    width = tokens.shape[2]
    count = tokens.shape[0]
    n_z, n_x, n_c = (lax.axis_size(a) for a in FS)
    own_rows = count // (n_z * n_x * n_c)
    row = jnp.arange(count, dtype=jnp.int32)
    c_at = (row // (count // n_c) + lax.axis_index("fs_2")) % n_c
    x_at = (row // (count // n_c // n_x) + lax.axis_index("fs_1")) % n_x
    z_at = (row // own_rows) % n_z
    source = ((z_at * n_x + x_at) * n_c + c_at) * own_rows + row % own_rows
    pick = source[:, None] == row[None, :]

    token_rows = tokens.reshape(count, width).astype(jnp.float32)
    row_mean = jnp.mean(token_rows, axis=1, keepdims=True)
    centered = token_rows - row_mean
    variance = jnp.mean(centered * centered, axis=1, keepdims=True)
    normed = (centered * lax.rsqrt(variance + norm_eps)).astype(jnp.bfloat16)
    normed = jnp.dot(pick.astype(jnp.bfloat16), normed, preferred_element_type=jnp.float32)
    normed = normed.astype(jnp.bfloat16)
    route_ids = expert_ids.reshape(-1, 2)
    route_mix = expert_mix.reshape(-1, 2)
    experts = gate_weight.shape[0]
    expert_iota = jnp.arange(experts, dtype=jnp.int32)
    expert_gates = jnp.sum(
        (route_ids[:, :, None] == expert_iota[None, None, :]).astype(jnp.float32)
        * route_mix[:, :, None],
        axis=1,
    )
    expert_gates = jnp.dot(pick.astype(jnp.float32), expert_gates, precision=lax.Precision.HIGHEST)

    gate_all, gate_act = acted(gate_pieces[0], normed, gate_pieces[1])
    up_all, hidden = acted(up_pieces[0], normed, up_pieces[1], gate_act, expert_gates)
    units = up_all.shape[0] // experts

    down_parts, summed = [], []
    for slots, pieces in down_pieces:
        down_c, away = mixed_away(slots, hidden, pieces)
        down_parts.append(down_c)
        away = shifted(away, "fs_2", 1)
        blocks = list(mixed_here(hidden, down_c, away, n_x))
        for s in range(1, n_x):
            blocks[s] = shifted(blocks[s], "fs_1", s)
        summed.append(blocks)
    pieces = folded(summed, n_z)
    pieces = lax.all_to_all(pieces, "fs_0", split_axis=0, concat_axis=0, tiled=True)
    mixed = finished(pieces)[:, None, :]
    down_all = jnp.concatenate(down_parts, axis=1)

    def as_served(a):
        return jnp.transpose(a.reshape(experts, units, width), (0, 2, 1))

    return (as_served(gate_all), as_served(up_all), as_served(down_all), mixed)


def solution(mesh):
    finer = Mesh(mesh.devices.reshape(8, 4, 2, mesh.shape["tp"]), ("fs_0", "fs_1", "fs_2", "tp"))
    placed_as = (
        P(None, "tp", None),
        P(FS),
        P(None, FS, "tp"),
        P(None, FS, "tp"),
        P(None, FS, "tp"),
        P(None, "tp", None),
        P(None, "tp", None),
    )
    return jax.shard_map(
        local,
        mesh=finer,
        in_specs=placed_as,
        out_specs=(P(None, None, FS), P(None, None, FS), P(None, None, FS), P(FS, "tp", None)),
        check_vma=False,
    )
```

profile of v0, /device:TPU:1, one launch (start us, length us, event | category | flops | bytes accessed | tf_op | source)
XLA Modules:
  0.0 182.5 jit_solution(18315432725778555829)
XLA Ops:
  0.6 1.2 copy-done.1
  1.9 1.2 copy-done.2
  3.1 0.7 copy-done.3
  3.7 1.5 prepare.2
  5.3 2.2 %collective-permute-start = (bf16[16,2,32,128]{3,2,1,0:T(8,128)(2,1)S(1)}, bf16[16,2,32,128]{3,2,1,0:T(8,128)(2,1)S(1)}, u32[]{:S(2)}, u32[]{:S(2)}) collective-permute-start(bf16[16,2,32,128]{3,2,1,0:T(8,128)(2,1)S(1)} %get-tuple-element.33), channel_id=1, source_target_pairs={{0,1},{1,2},{2,3},{3,0},{4,5},{5,6},{6,7},{7,4},{8,9},{9,10},{10,1... | collective-permute-start | bytes 786440 | tf_op jit(solution)/shard_map/ppermute | solution.py:22
  7.5 2.6 %collective-permute-start.1 = (bf16[16,2,32,128]{3,2,1,0:T(8,128)(2,1)S(1)}, bf16[16,2,32,128]{3,2,1,0:T(8,128)(2,1)S(1)}, u32[]{:S(2)}, u32[]{:S(2)}) collective-permute-start(bf16[16,2,32,128]{3,2,1,0:T(8,128)(2,1)S(1)} %get-tuple-element.34), channel_id=1, source_target_pairs={{0,2},{1,3},{2,0},{3,1},{4,6},{5,7},{6,4},{7,5},{8,10},{9,11},{10,... | collective-permute-start | bytes 786440 | tf_op jit(solution)/shard_map/ppermute | solution.py:22
  10.1 1.1 collective-permute-start.2
  11.1 0.1 pad_add_fusion.1.slot_ref
  11.2 1.8 collective-permute-done.refs_1_
  13.0 8.4 %collective-permute-done.1.refs_2_ = bf16[16,2,32,128]{3,2,1,0:T(8,128)(2,1)S(1)} collective-permute-done((bf16[16,2,32,128]{3,2,1,0:T(8,128)(2,1)S(1)}, bf16[16,2,32,128]{3,2,1,0:T(8,128)(2,1)S(1)}, u32[]{:S(2)}, u32[]{:S(2)}) %collective-permute-start.1) | collective-permute-done | bytes 262176 | tf_op jit(solution)/shard_map/ppermute | solution.py:22
  21.4 1.6 placed.2
  23.0 13.0 %all-to-all-start = ((bf16[64,2,32,128]{3,2,1,0:T(8,128)(2,1)}), bf16[64,2,32,128]{3,2,1,0:T(8,128)(2,1)S(1)}, u32[]{:S(2)}, u32[]{:S(2)}) async-start(bf16[64,2,32,128]{3,2,1,0:T(8,128)(2,1)} %bitcast.11), calls=%async_computation | async-start | bytes 2097152 | tf_op jit(solution)/shard_map/all_to_all | solution.py:307
  36.0 1.3 prepare.3
  37.3 1.0 collective-permute-start.9
  38.4 2.1 %collective-permute-start.10 = (bf16[16,1,32,128]{3,2,1,0:T(8,128)(2,1)S(1)}, bf16[16,1,32,128]{3,2,1,0:T(8,128)(2,1)S(1)}, u32[]{:S(2)}, u32[]{:S(2)}) collective-permute-start(bf16[16,1,32,128]{3,2,1,0:T(8,128)(2,1)S(1)} %get-tuple-element.44), channel_id=1, source_target_pairs={{0,2},{1,3},{2,0},{3,1},{4,6},{5,7},{6,4},{7,5},{8,10},{9,11},{10,... | collective-permute-start | bytes 393224 | tf_op jit(solution)/shard_map/ppermute | solution.py:22
  40.5 1.3 collective-permute-start.11
  41.8 1.4 collective-permute-done.9.refs_1_
  43.2 3.2 %collective-permute-done.10.refs_2_ = bf16[16,1,32,128]{3,2,1,0:T(8,128)(2,1)S(1)} collective-permute-done((bf16[16,1,32,128]{3,2,1,0:T(8,128)(2,1)S(1)}, bf16[16,1,32,128]{3,2,1,0:T(8,128)(2,1)S(1)}, u32[]{:S(2)}, u32[]{:S(2)}) %collective-permute-start.10) | collective-permute-done | bytes 131104 | tf_op jit(solution)/shard_map/ppermute | solution.py:22
  46.4 1.4 placed.3
  47.8 16.4 %all-to-all-done.x_ref = bf16[64,2,32,128]{3,2,1,0:T(8,128)(2,1)S(1)} async-done(((bf16[64,2,32,128]{3,2,1,0:T(8,128)(2,1)}), bf16[64,2,32,128]{3,2,1,0:T(8,128)(2,1)S(1)}, u32[]{:S(2)}, u32[]{:S(2)}) %all-to-all-start) | async-done | bytes 1048608 | tf_op jit(solution)/shard_map/all_to_all | solution.py:307
  64.2 6.3 %all-to-all-start.1 = ((bf16[64,1,32,128]{3,2,1,0:T(8,128)(2,1)}), bf16[64,1,32,128]{3,2,1,0:T(8,128)(2,1)S(1)}, u32[]{:S(2)}, u32[]{:S(2)}) async-start(bf16[64,1,32,128]{3,2,1,0:T(8,128)(2,1)} %bitcast.18), calls=%async_computation.1 | async-start | bytes 1048576 | tf_op jit(solution)/shard_map/all_to_all | solution.py:307
  70.5 2.5 %convert_reduce_fusion = f32[768]{0:T(1024)S(1)} fusion(bf16[768,1,2048]{2,0,1:T(8,128)(2,1)} %param.7), kind=kLoop, calls=%fused_computation | loop fusion | flops 3144960 | bytes 3148800 | tf_op jit(solution)/shard_map/reduce_sum | solution.py:329
  73.0 2.0 %turned.2 = (bf16[128,2048]{1,0:T(8,128)(2,1)}, bf16[128,2048]{1,0:T(8,128)(2,1)}) custom-call(bf16[64,2,32,128]{3,2,1,0:T(8,128)(2,1)S(1)} %all-to-all-done.x_ref), custom_call_target="tpu_custom_call" | custom-call | tf_op jit(solution)/shard_map/turned/pallas_call | solution.py:156
  75.0 1.0 collective-permute-start.3
  76.0 1.7 collective-permute-start.7
  77.7 1.0 fusion.3
  78.7 9.5 %all-to-all-done.1.x_ref = bf16[64,1,32,128]{3,2,1,0:T(8,128)(2,1)S(1)} async-done(((bf16[64,1,32,128]{3,2,1,0:T(8,128)(2,1)}), bf16[64,1,32,128]{3,2,1,0:T(8,128)(2,1)S(1)}, u32[]{:S(2)}, u32[]{:S(2)}) %all-to-all-start.1) | async-done | bytes 524320 | tf_op jit(solution)/shard_map/all_to_all | solution.py:307
  88.2 1.2 turned.3
  89.4 1.0 collective-permute-start.12
  90.3 1.7 collective-permute-start.4
  92.0 0.8 collective-permute-start.5
  92.8 2.0 %collective-permute-start.8 = (bf16[128,2048]{1,0:T(8,128)(2,1)}, bf16[128,2048]{1,0:T(8,128)(2,1)}, u32[]{:S(2)}, u32[]{:S(2)}) collective-permute-start(bf16[128,2048]{1,0:T(8,128)(2,1)} %collective-permute-done.7.refs_2_), channel_id=1, source_target_pairs={{0,3},{1,0},{2,1},{3,2},{4,7},{5,4},{6,5},{7,6},{8,11},{9,8},{10,9... | collective-permute-start | bytes 1572872 | tf_op jit(solution)/shard_map/ppermute | solution.py:22
  94.8 4.8 %convolution_convert_fusion.n_ref = bf16[768,2048]{1,0:T(8,128)(2,1)S(1)} fusion(bf16[768,1,2048]{2,0,1:T(8,128)(2,1)} %param.7, f32[768]{0:T(1024)S(1)} %add_rsqrt_fusion, f32[768]{0:T(1024)S(1)} %broadcast_multiply_fusion, s32[768]{0:T(1024)S(1)} %fusion.25), kind=kOutput, calls=%fused_computation.7 | convolution fusion | flops 2424373248 | bytes 6300672 | tf_op jit(solution)/shard_map/dot_general | solution.py:333
  99.6 1.5 collective-permute-start.13
  101.1 2.3 %collective-permute-done.4.refs_2_ = bf16[128,2048]{1,0:T(8,128)(2,1)} collective-permute-done((bf16[128,2048]{1,0:T(8,128)(2,1)}, bf16[128,2048]{1,0:T(8,128)(2,1)}, u32[]{:S(2)}, u32[]{:S(2)}) %collective-permute-start.4) | collective-permute-done | bytes 524320 | tf_op jit(solution)/shard_map/ppermute | solution.py:22
  103.4 2.1 %collective-permute-start.14 = (bf16[128,1024]{1,0:T(8,128)(2,1)}, bf16[128,1024]{1,0:T(8,128)(2,1)S(1)}, u32[]{:S(2)}, u32[]{:S(2)}) collective-permute-start(bf16[128,1024]{1,0:T(8,128)(2,1)} %get-tuple-element.46.refs_0_), channel_id=1, source_target_pairs={{0,2},{1,3},{2,0},{3,1},{4,6},{5,7},{6,4},{7,5},{8,10},{9,11},{10,... | collective-permute-start | bytes 786440 | tf_op jit(solution)/shard_map/ppermute | solution.py:22
  105.6 1.2 fusion.8.refs_5_
  106.7 2.9 %collective-permute-done.6.refs_1_ = bf16[128,2048]{1,0:T(8,128)(2,1)} collective-permute-done((bf16[128,2048]{1,0:T(8,128)(2,1)}, bf16[128,2048]{1,0:T(8,128)(2,1)}, u32[]{:S(2)}, u32[]{:S(2)}) %collective-permute-start.6) | collective-permute-done | bytes 524320 | tf_op jit(solution)/shard_map/ppermute | solution.py:22
  109.6 11.2 %collective-permute-done.5.refs_3_ = bf16[128,2048]{1,0:T(8,128)(2,1)} collective-permute-done((bf16[128,2048]{1,0:T(8,128)(2,1)}, bf16[128,2048]{1,0:T(8,128)(2,1)}, u32[]{:S(2)}, u32[]{:S(2)}) %collective-permute-start.5) | collective-permute-done | bytes 524320 | tf_op jit(solution)/shard_map/ppermute | solution.py:22
  120.8 0.7 collective-permute-start.16
  121.5 0.9 collective-permute-start.17
  122.4 4.0 %acted.2 = (bf16[512,2048]{1,0:T(8,128)(2,1)}, f32[768,512]{1,0:T(8,128)S(1)}) custom-call(s32[4]{0:T(128)S(1)} %pad_add_fusion.slot_ref, bf16[768,2048]{1,0:T(8,128)(2,1)S(1)} %convolution_convert_fusion.n_ref, bf16[128,2048]{1,0:T(8,128)(2,1)} %get-tuple-element.36.refs_0_, bf16[128,2048]{1,0:T(8,128)(2,1)} %collective-permute-done.3.refs_1_, ...), custom_call_target="tpu_custom_call" | custom-call | tf_op jit(solution)/shard_map/acted/pallas_call | solution.py:127
  126.4 4.1 %acted.3 = (bf16[512,2048]{1,0:T(8,128)(2,1)}, bf16[768,512]{1,0:T(8,128)(2,1)S(1)}) custom-call(s32[4]{0:T(128)S(1)} %pad_add_fusion.slot_ref, bf16[768,2048]{1,0:T(8,128)(2,1)S(1)} %convolution_convert_fusion.n_ref, bf16[128,2048]{1,0:T(8,128)(2,1)} %get-tuple-element.38.refs_0_, bf16[128,2048]{1,0:T(8,128)(2,1)} %collective-permute-done.6.refs_1_, ...), custom_call_target="tpu_custom_call" | custom-call | tf_op jit(solution)/shard_map/acted/pallas_call | solution.py:127
  130.6 2.2 %mixed_away.2 = (bf16[512,1024]{1,0:T(8,128)(2,1)S(1)}, bf16[384,1024]{1,0:T(8,128)(2,1)S(1)}) custom-call(s32[4]{0:T(128)S(1)} %pad_add_fusion.slot_ref, bf16[768,512]{1,0:T(8,128)(2,1)S(1)} %get-tuple-element.41.h_ref, bf16[128,1024]{1,0:T(8,128)(2,1)} %get-tuple-element.46.refs_0_, bf16[128,1024]{1,0:T(8,128)(2,1)} %collective-permute-done.12.refs_1_, ...), custom_call_target="tpu_custom_call" | custom-call | tf_op jit(solution)/shard_map/mixed_away/pallas_call | solution.py:200
  132.8 7.6 %collective-permute-start.18 = (bf16[384,1024]{1,0:T(8,128)(2,1)S(1)}, bf16[384,1024]{1,0:T(8,128)(2,1)S(1)}, u32[]{:S(2)}, u32[]{:S(2)}) collective-permute-start(bf16[384,1024]{1,0:T(8,128)(2,1)S(1)} %get-tuple-element.50), channel_id=1, source_target_pairs={{0,4},{4,0},{1,5},{5,1},{2,6},{6,2},{3,7},{7,3},{8,12},{12,8},{9,1... | collective-permute-start | bytes 2359304 | tf_op jit(solution)/shard_map/ppermute | solution.py:22
  140.4 1.7 mixed_away.3
  142.1 0.1 collective-permute-start.22
  142.3 1.1 mixed_here.2
  143.4 1.3 collective-permute-start.19
  144.7 2.4 %collective-permute-start.20 = (bf16[96,1024]{1,0:T(8,128)(2,1)S(1)}, bf16[96,1024]{1,0:T(8,128)(2,1)S(1)}, u32[]{:S(2)}, u32[]{:S(2)}) collective-permute-start(bf16[96,1024]{1,0:T(8,128)(2,1)S(1)} %get-tuple-element.53), channel_id=1, source_target_pairs={{0,16},{8,24},{16,0},{24,8},{1,17},{9,25},{17,1},{25,9},{2,18},{10... | collective-permute-start | bytes 589832 | tf_op jit(solution)/shard_map/ppermute | solution.py:22
  147.1 1.2 collective-permute-start.21
  148.3 1.1 mixed_here.3
  149.4 0.4 collective-permute-start.23
  149.8 0.9 collective-permute-start.24
  150.6 0.1 collective-permute-done.19.refs_1_
  150.7 1.5 collective-permute-start.25
  152.3 3.7 %collective-permute-done.20.refs_2_ = bf16[96,1024]{1,0:T(8,128)(2,1)S(1)} collective-permute-done((bf16[96,1024]{1,0:T(8,128)(2,1)S(1)}, bf16[96,1024]{1,0:T(8,128)(2,1)S(1)}, u32[]{:S(2)}, u32[]{:S(2)}) %collective-permute-start.20) | collective-permute-done | bytes 196640 | tf_op jit(solution)/shard_map/ppermute | solution.py:22
  155.9 5.6 %collective-permute-done.23.refs_5_ = bf16[96,1024]{1,0:T(8,128)(2,1)S(1)} collective-permute-done((bf16[96,1024]{1,0:T(8,128)(2,1)S(1)}, bf16[96,1024]{1,0:T(8,128)(2,1)S(1)}, u32[]{:S(2)}, u32[]{:S(2)}) %collective-permute-start.23) | collective-permute-done | bytes 196640 | tf_op jit(solution)/shard_map/ppermute | solution.py:22
  161.5 2.9 %collective-permute-done.24.refs_6_ = bf16[96,1024]{1,0:T(8,128)(2,1)S(1)} collective-permute-done((bf16[96,1024]{1,0:T(8,128)(2,1)S(1)}, bf16[96,1024]{1,0:T(8,128)(2,1)S(1)}, u32[]{:S(2)}, u32[]{:S(2)}) %collective-permute-start.24) | collective-permute-done | bytes 196640 | tf_op jit(solution)/shard_map/ppermute | solution.py:22
  164.4 1.0 folded.1
  165.4 3.6 %all-to-all-start.2 = ((bf16[8,24,1024]{2,1,0:T(8,128)(2,1)}), bf16[8,24,1024]{2,1,0:T(8,128)(2,1)S(1)}, u32[]{:S(2)}, u32[]{:S(2)}) async-start(bf16[8,24,1024]{2,1,0:T(8,128)(2,1)} %folded.1), calls=%async_computation.2 | async-start | bytes 786432 | tf_op jit(solution)/shard_map/all_to_all | solution.py:360
  169.0 1.5 pad_maximum_fusion
  170.5 11.3 %all-to-all-done.2.p_ref = bf16[8,24,1024]{2,1,0:T(8,128)(2,1)S(1)} async-done(((bf16[8,24,1024]{2,1,0:T(8,128)(2,1)}), bf16[8,24,1024]{2,1,0:T(8,128)(2,1)S(1)}, u32[]{:S(2)}, u32[]{:S(2)}) %all-to-all-start.2) | async-done | bytes 393248 | tf_op jit(solution)/shard_map/all_to_all | solution.py:360
  181.8 0.7 finished.1
  (35 shorter events, 0.3 us)
Async XLA Ops:
  0.6 1.2 copy-start.1
  1.9 1.2 copy-start.2
  3.1 0.7 copy-start.3
  3.7 32.3 %copy-start = (f32[8,32,1024]{2,1,0:T(8,128)S(1)}, f32[8,32,1024]{2,1,0:T(8,128)}, u32[]{:S(2)}) copy-start(f32[8,32,1024]{2,1,0:T(8,128)} %refs_0_.3) | copy-start | bytes 3145732
  3.7 32.3 %copy-start.4 = (f32[32]{0:T(128)S(1)}, f32[32]{0:T(128)}, u32[]{:S(2)}) copy-start(f32[32]{0:T(128)} %param.8) | copy-start | bytes 388
  5.3 7.7 %collective-permute-start = (bf16[16,2,32,128]{3,2,1,0:T(8,128)(2,1)S(1)}, bf16[16,2,32,128]{3,2,1,0:T(8,128)(2,1)S(1)}, u32[]{:S(2)}, u32[]{:S(2)}) collective-permute-start(bf16[16,2,32,128]{3,2,1,0:T(8,128)(2,1)S(1)} %get-tuple-element.33), channel_id=1, source_target_pairs={{0,1},{1,2},{2,3},{3,0},{4,5},{5,6},{6,7},{7,4},{8,9},{9,10},{10,1... | collective-permute-start | bytes 786440 | tf_op jit(solution)/shard_map/ppermute | solution.py:22
  7.5 14.0 %collective-permute-start.1 = (bf16[16,2,32,128]{3,2,1,0:T(8,128)(2,1)S(1)}, bf16[16,2,32,128]{3,2,1,0:T(8,128)(2,1)S(1)}, u32[]{:S(2)}, u32[]{:S(2)}) collective-permute-start(bf16[16,2,32,128]{3,2,1,0:T(8,128)(2,1)S(1)} %get-tuple-element.34), channel_id=1, source_target_pairs={{0,2},{1,3},{2,0},{3,1},{4,6},{5,7},{6,4},{7,5},{8,10},{9,11},{10,... | collective-permute-start | bytes 786440 | tf_op jit(solution)/shard_map/ppermute | solution.py:22
  10.1 11.3 %collective-permute-start.2 = (bf16[16,2,32,128]{3,2,1,0:T(8,128)(2,1)S(1)}, bf16[16,2,32,128]{3,2,1,0:T(8,128)(2,1)S(1)}, u32[]{:S(2)}, u32[]{:S(2)}) collective-permute-start(bf16[16,2,32,128]{3,2,1,0:T(8,128)(2,1)S(1)} %get-tuple-element.35), channel_id=1, source_target_pairs={{0,3},{1,0},{2,1},{3,2},{4,7},{5,4},{6,5},{7,6},{8,11},{9,8},{10,9... | collective-permute-start | bytes 786440 | tf_op jit(solution)/shard_map/ppermute | solution.py:22
  23.0 41.2 %all-to-all-start = ((bf16[64,2,32,128]{3,2,1,0:T(8,128)(2,1)}), bf16[64,2,32,128]{3,2,1,0:T(8,128)(2,1)S(1)}, u32[]{:S(2)}, u32[]{:S(2)}) async-start(bf16[64,2,32,128]{3,2,1,0:T(8,128)(2,1)} %bitcast.11), calls=%async_computation | async-start | bytes 2097152 | tf_op jit(solution)/shard_map/all_to_all | solution.py:307
  37.3 5.9 %collective-permute-start.9 = (bf16[16,1,32,128]{3,2,1,0:T(8,128)(2,1)S(1)}, bf16[16,1,32,128]{3,2,1,0:T(8,128)(2,1)S(1)}, u32[]{:S(2)}, u32[]{:S(2)}) collective-permute-start(bf16[16,1,32,128]{3,2,1,0:T(8,128)(2,1)S(1)} %get-tuple-element.43), channel_id=1, source_target_pairs={{0,1},{1,2},{2,3},{3,0},{4,5},{5,6},{6,7},{7,4},{8,9},{9,10},{10,1... | collective-permute-start | bytes 393224 | tf_op jit(solution)/shard_map/ppermute | solution.py:22
  38.4 8.1 %collective-permute-start.10 = (bf16[16,1,32,128]{3,2,1,0:T(8,128)(2,1)S(1)}, bf16[16,1,32,128]{3,2,1,0:T(8,128)(2,1)S(1)}, u32[]{:S(2)}, u32[]{:S(2)}) collective-permute-start(bf16[16,1,32,128]{3,2,1,0:T(8,128)(2,1)S(1)} %get-tuple-element.44), channel_id=1, source_target_pairs={{0,2},{1,3},{2,0},{3,1},{4,6},{5,7},{6,4},{7,5},{8,10},{9,11},{10,... | collective-permute-start | bytes 393224 | tf_op jit(solution)/shard_map/ppermute | solution.py:22
  40.5 5.9 %collective-permute-start.11 = (bf16[16,1,32,128]{3,2,1,0:T(8,128)(2,1)S(1)}, bf16[16,1,32,128]{3,2,1,0:T(8,128)(2,1)S(1)}, u32[]{:S(2)}, u32[]{:S(2)}) collective-permute-start(bf16[16,1,32,128]{3,2,1,0:T(8,128)(2,1)S(1)} %get-tuple-element.45), channel_id=1, source_target_pairs={{0,3},{1,0},{2,1},{3,2},{4,7},{5,4},{6,5},{7,6},{8,11},{9,8},{10,9... | collective-permute-start | bytes 393224 | tf_op jit(solution)/shard_map/ppermute | solution.py:22
  64.2 24.0 %all-to-all-start.1 = ((bf16[64,1,32,128]{3,2,1,0:T(8,128)(2,1)}), bf16[64,1,32,128]{3,2,1,0:T(8,128)(2,1)S(1)}, u32[]{:S(2)}, u32[]{:S(2)}) async-start(bf16[64,1,32,128]{3,2,1,0:T(8,128)(2,1)} %bitcast.18), calls=%async_computation.1 | async-start | bytes 1048576 | tf_op jit(solution)/shard_map/all_to_all | solution.py:307
  70.5 7.3 %copy-start.5 = (bf16[768,1,2048]{2,0,1:T(8,128)(2,1)S(1)}, bf16[768,1,2048]{2,0,1:T(8,128)(2,1)}, u32[]{:S(2)}) copy-start(bf16[768,1,2048]{2,0,1:T(8,128)(2,1)} %param.7) | copy-start | bytes 9437188
  75.0 17.0 %collective-permute-start.3 = (bf16[128,2048]{1,0:T(8,128)(2,1)}, bf16[128,2048]{1,0:T(8,128)(2,1)}, u32[]{:S(2)}, u32[]{:S(2)}) collective-permute-start(bf16[128,2048]{1,0:T(8,128)(2,1)} %get-tuple-element.36.refs_0_), channel_id=1, source_target_pairs={{0,1},{1,2},{2,3},{3,0},{4,5},{5,6},{6,7},{7,4},{8,9},{9,10},{10,1... | collective-permute-start | bytes 1572872 | tf_op jit(solution)/shard_map/ppermute | solution.py:22
  76.0 16.8 %collective-permute-start.7 = (bf16[128,2048]{1,0:T(8,128)(2,1)}, bf16[128,2048]{1,0:T(8,128)(2,1)}, u32[]{:S(2)}, u32[]{:S(2)}) collective-permute-start(bf16[128,2048]{1,0:T(8,128)(2,1)} %get-tuple-element.38.refs_0_), channel_id=1, source_target_pairs={{0,3},{1,0},{2,1},{3,2},{4,7},{5,4},{6,5},{7,6},{8,11},{9,8},{10,9... | collective-permute-start | bytes 1572872 | tf_op jit(solution)/shard_map/ppermute | solution.py:22
  89.4 10.2 %copy-start.6 = (f32[768,1,2]{0,2,1:T(2,128)S(1)}, f32[768,1,2]{0,2,1:T(2,128)}, u32[]{:S(2)}) copy-start(f32[768,1,2]{0,2,1:T(2,128)} %param.13) | copy-start | bytes 18436
  89.4 10.2 %copy-start.7 = (s32[768,1,2]{0,2,1:T(2,128)S(1)}, s32[768,1,2]{0,2,1:T(2,128)}, u32[]{:S(2)}) copy-start(s32[768,1,2]{0,2,1:T(2,128)} %param.12) | copy-start | bytes 18436
  89.4 10.3 %collective-permute-start.12 = (bf16[128,1024]{1,0:T(8,128)(2,1)}, bf16[128,1024]{1,0:T(8,128)(2,1)}, u32[]{:S(2)}, u32[]{:S(2)}) collective-permute-start(bf16[128,1024]{1,0:T(8,128)(2,1)} %get-tuple-element.46.refs_0_), channel_id=1, source_target_pairs={{0,1},{1,2},{2,3},{3,0},{4,5},{5,6},{6,7},{7,4},{8,9},{9,10},{10,1... | collective-permute-start | bytes 786440 | tf_op jit(solution)/shard_map/ppermute | solution.py:22
  90.3 13.1 %collective-permute-start.4 = (bf16[128,2048]{1,0:T(8,128)(2,1)}, bf16[128,2048]{1,0:T(8,128)(2,1)}, u32[]{:S(2)}, u32[]{:S(2)}) collective-permute-start(bf16[128,2048]{1,0:T(8,128)(2,1)} %get-tuple-element.36.refs_0_), channel_id=1, source_target_pairs={{0,3},{1,0},{2,1},{3,2},{4,7},{5,4},{6,5},{7,6},{8,11},{9,8},{10,9... | collective-permute-start | bytes 1572872 | tf_op jit(solution)/shard_map/ppermute | solution.py:22
  92.0 17.6 %collective-permute-start.6 = (bf16[128,2048]{1,0:T(8,128)(2,1)}, bf16[128,2048]{1,0:T(8,128)(2,1)}, u32[]{:S(2)}, u32[]{:S(2)}) collective-permute-start(bf16[128,2048]{1,0:T(8,128)(2,1)} %get-tuple-element.38.refs_0_), channel_id=1, source_target_pairs={{0,1},{1,2},{2,3},{3,0},{4,5},{5,6},{6,7},{7,4},{8,9},{9,10},{10,1... | collective-permute-start | bytes 1572872 | tf_op jit(solution)/shard_map/ppermute | solution.py:22
  92.0 28.8 %collective-permute-start.5 = (bf16[128,2048]{1,0:T(8,128)(2,1)}, bf16[128,2048]{1,0:T(8,128)(2,1)}, u32[]{:S(2)}, u32[]{:S(2)}) collective-permute-start(bf16[128,2048]{1,0:T(8,128)(2,1)} %collective-permute-done.3.refs_1_), channel_id=1, source_target_pairs={{0,1},{1,2},{2,3},{3,0},{4,5},{5,6},{6,7},{7,4},{8,9},{9,10},{10,1... | collective-permute-start | bytes 1572872 | tf_op jit(solution)/shard_map/ppermute | solution.py:22
  92.8 28.7 %collective-permute-start.8 = (bf16[128,2048]{1,0:T(8,128)(2,1)}, bf16[128,2048]{1,0:T(8,128)(2,1)}, u32[]{:S(2)}, u32[]{:S(2)}) collective-permute-start(bf16[128,2048]{1,0:T(8,128)(2,1)} %collective-permute-done.7.refs_2_), channel_id=1, source_target_pairs={{0,3},{1,0},{2,1},{3,2},{4,7},{5,4},{6,5},{7,6},{8,11},{9,8},{10,9... | collective-permute-start | bytes 1572872 | tf_op jit(solution)/shard_map/ppermute | solution.py:22
  99.6 30.9 %collective-permute-start.13 = (bf16[128,1024]{1,0:T(8,128)(2,1)}, bf16[128,1024]{1,0:T(8,128)(2,1)S(1)}, u32[]{:S(2)}, u32[]{:S(2)}) collective-permute-start(bf16[128,1024]{1,0:T(8,128)(2,1)} %get-tuple-element.46.refs_0_), channel_id=1, source_target_pairs={{0,3},{1,0},{2,1},{3,2},{4,7},{5,4},{6,5},{7,6},{8,11},{9,8},{10,9... | collective-permute-start | bytes 786440 | tf_op jit(solution)/shard_map/ppermute | solution.py:22
  103.4 27.1 %collective-permute-start.14 = (bf16[128,1024]{1,0:T(8,128)(2,1)}, bf16[128,1024]{1,0:T(8,128)(2,1)S(1)}, u32[]{:S(2)}, u32[]{:S(2)}) collective-permute-start(bf16[128,1024]{1,0:T(8,128)(2,1)} %get-tuple-element.46.refs_0_), channel_id=1, source_target_pairs={{0,2},{1,3},{2,0},{3,1},{4,6},{5,7},{6,4},{7,5},{8,10},{9,11},{10,... | collective-permute-start | bytes 786440 | tf_op jit(solution)/shard_map/ppermute | solution.py:22
  109.6 30.8 %collective-permute-start.15 = (bf16[128,1024]{1,0:T(8,128)(2,1)S(1)}, bf16[128,1024]{1,0:T(8,128)(2,1)S(1)}, u32[]{:S(2)}, u32[]{:S(2)}) collective-permute-start(bf16[128,1024]{1,0:T(8,128)(2,1)S(1)} %get-tuple-element.48.refs_0_), channel_id=1, source_target_pairs={{0,1},{1,2},{2,3},{3,0},{4,5},{5,6},{6,7},{7,4},{8,9},{9,10},{10,1... | collective-permute-start | bytes 786440 | tf_op jit(solution)/shard_map/ppermute | solution.py:22
  120.8 19.6 %collective-permute-start.16 = (bf16[128,1024]{1,0:T(8,128)(2,1)S(1)}, bf16[128,1024]{1,0:T(8,128)(2,1)S(1)}, u32[]{:S(2)}, u32[]{:S(2)}) collective-permute-start(bf16[128,1024]{1,0:T(8,128)(2,1)S(1)} %get-tuple-element.48.refs_0_), channel_id=1, source_target_pairs={{0,3},{1,0},{2,1},{3,2},{4,7},{5,4},{6,5},{7,6},{8,11},{9,8},{10,9... | collective-permute-start | bytes 786440 | tf_op jit(solution)/shard_map/ppermute | solution.py:22
  121.5 18.9 %collective-permute-start.17 = (bf16[128,1024]{1,0:T(8,128)(2,1)S(1)}, bf16[128,1024]{1,0:T(8,128)(2,1)S(1)}, u32[]{:S(2)}, u32[]{:S(2)}) collective-permute-start(bf16[128,1024]{1,0:T(8,128)(2,1)S(1)} %get-tuple-element.48.refs_0_), channel_id=1, source_target_pairs={{0,2},{1,3},{2,0},{3,1},{4,6},{5,7},{6,4},{7,5},{8,10},{9,11},{10,... | collective-permute-start | bytes 786440 | tf_op jit(solution)/shard_map/ppermute | solution.py:22
  132.8 9.6 %collective-permute-start.18 = (bf16[384,1024]{1,0:T(8,128)(2,1)S(1)}, bf16[384,1024]{1,0:T(8,128)(2,1)S(1)}, u32[]{:S(2)}, u32[]{:S(2)}) collective-permute-start(bf16[384,1024]{1,0:T(8,128)(2,1)S(1)} %get-tuple-element.50), channel_id=1, source_target_pairs={{0,4},{4,0},{1,5},{5,1},{2,6},{6,2},{3,7},{7,3},{8,12},{12,8},{9,1... | collective-permute-start | bytes 2359304 | tf_op jit(solution)/shard_map/ppermute | solution.py:22
  142.1 6.1 %collective-permute-start.22 = (bf16[384,1024]{1,0:T(8,128)(2,1)S(1)}, bf16[384,1024]{1,0:T(8,128)(2,1)S(1)}, u32[]{:S(2)}, u32[]{:S(2)}) collective-permute-start(bf16[384,1024]{1,0:T(8,128)(2,1)S(1)} %get-tuple-element.55), channel_id=1, source_target_pairs={{0,4},{4,0},{1,5},{5,1},{2,6},{6,2},{3,7},{7,3},{8,12},{12,8},{9,1... | collective-permute-start | bytes 2359304 | tf_op jit(solution)/shard_map/ppermute | solution.py:22
  143.4 7.3 %collective-permute-start.19 = (bf16[96,1024]{1,0:T(8,128)(2,1)S(1)}, bf16[96,1024]{1,0:T(8,128)(2,1)S(1)}, u32[]{:S(2)}, u32[]{:S(2)}) collective-permute-start(bf16[96,1024]{1,0:T(8,128)(2,1)S(1)} %get-tuple-element.52), channel_id=1, source_target_pairs={{0,8},{8,16},{16,24},{24,0},{1,9},{9,17},{17,25},{25,1},{2,10},{10... | collective-permute-start | bytes 589832 | tf_op jit(solution)/shard_map/ppermute | solution.py:22
  144.7 11.2 %collective-permute-start.20 = (bf16[96,1024]{1,0:T(8,128)(2,1)S(1)}, bf16[96,1024]{1,0:T(8,128)(2,1)S(1)}, u32[]{:S(2)}, u32[]{:S(2)}) collective-permute-start(bf16[96,1024]{1,0:T(8,128)(2,1)S(1)} %get-tuple-element.53), channel_id=1, source_target_pairs={{0,16},{8,24},{16,0},{24,8},{1,17},{9,25},{17,1},{25,9},{2,18},{10... | collective-permute-start | bytes 589832 | tf_op jit(solution)/shard_map/ppermute | solution.py:22
  147.1 8.8 %collective-permute-start.21 = (bf16[96,1024]{1,0:T(8,128)(2,1)S(1)}, bf16[96,1024]{1,0:T(8,128)(2,1)S(1)}, u32[]{:S(2)}, u32[]{:S(2)}) collective-permute-start(bf16[96,1024]{1,0:T(8,128)(2,1)S(1)} %get-tuple-element.54), channel_id=1, source_target_pairs={{0,24},{8,0},{16,8},{24,16},{1,25},{9,1},{17,9},{25,17},{2,26},{10... | collective-permute-start | bytes 589832 | tf_op jit(solution)/shard_map/ppermute | solution.py:22
  149.4 12.1 %collective-permute-start.23 = (bf16[96,1024]{1,0:T(8,128)(2,1)S(1)}, bf16[96,1024]{1,0:T(8,128)(2,1)S(1)}, u32[]{:S(2)}, u32[]{:S(2)}) collective-permute-start(bf16[96,1024]{1,0:T(8,128)(2,1)S(1)} %get-tuple-element.57), channel_id=1, source_target_pairs={{0,8},{8,16},{16,24},{24,0},{1,9},{9,17},{17,25},{25,1},{2,10},{10... | collective-permute-start | bytes 589832 | tf_op jit(solution)/shard_map/ppermute | solution.py:22
  149.8 14.6 %collective-permute-start.24 = (bf16[96,1024]{1,0:T(8,128)(2,1)S(1)}, bf16[96,1024]{1,0:T(8,128)(2,1)S(1)}, u32[]{:S(2)}, u32[]{:S(2)}) collective-permute-start(bf16[96,1024]{1,0:T(8,128)(2,1)S(1)} %get-tuple-element.58), channel_id=1, source_target_pairs={{0,16},{8,24},{16,0},{24,8},{1,17},{9,25},{17,1},{25,9},{2,18},{10... | collective-permute-start | bytes 589832 | tf_op jit(solution)/shard_map/ppermute | solution.py:22
  150.7 13.6 %collective-permute-start.25 = (bf16[96,1024]{1,0:T(8,128)(2,1)S(1)}, bf16[96,1024]{1,0:T(8,128)(2,1)S(1)}, u32[]{:S(2)}, u32[]{:S(2)}) collective-permute-start(bf16[96,1024]{1,0:T(8,128)(2,1)S(1)} %get-tuple-element.59), channel_id=1, source_target_pairs={{0,24},{8,0},{16,8},{24,16},{1,25},{9,1},{17,9},{25,17},{2,26},{10... | collective-permute-start | bytes 589832 | tf_op jit(solution)/shard_map/ppermute | solution.py:22
  165.4 16.4 %all-to-all-start.2 = ((bf16[8,24,1024]{2,1,0:T(8,128)(2,1)}), bf16[8,24,1024]{2,1,0:T(8,128)(2,1)S(1)}, u32[]{:S(2)}, u32[]{:S(2)}) async-start(bf16[8,24,1024]{2,1,0:T(8,128)(2,1)} %folded.1), calls=%async_computation.2 | async-start | bytes 786432 | tf_op jit(solution)/shard_map/all_to_all | solution.py:360
where the time goes:
time: 185 us; the launch traced here: 182 us
  waiting for transfers between devices  80.8 us (44%)
  starting transfers between devices  61.8 us (33%)
  Pallas kernels  24.9 us (13%)
  matrix products  5.93 us (3%)
  other arithmetic  5.18 us (3%)
  local copies, waits for them, and re-layouts  3.12 us (2%)
    ppermute x26, waiting for transfers between devices, shifted(): return lax.ppermute(array, axis, [(i, (i + by) % n) for i in range(n)])  43.6 us
    ppermute x26, starting transfers between devices, shifted(): return lax.ppermute(array, axis, [(i, (i + by) % n) for i in range(n)])  38.9 us
    all_to_all x2, waiting for transfers between devices, handed(): return lax.all_to_all(columns, FS, split_axis=0, concat_axis=0, tiled=True)  25.9 us
    all_to_all x2, starting transfers between devices, handed(): return lax.all_to_all(columns, FS, split_axis=0, concat_axis=0, tiled=True)  19.3 us
    all_to_all x1, waiting for transfers between devices, local(): lax.all_to_all(pieces, 'fs_0', split_axis=0, concat_axis=0, tiled=True)  11.3 us
    pallas_call x2, Pallas kernels, acted(): pl.pallas_call(body, out_shape=[jax.ShapeDtypeStruct((units, width), jnp....  8.1 us
    dot_general x1, matrix products, local(): jnp.dot(pick.astype(jnp.bfloat16), normed, preferred_element_type=jnp.flo...  4.76 us
    pallas_call x2, Pallas kernels, mixed_away(): pl.pallas_call(body, out_shape=[jax.ShapeDtypeStruct((units, wide), jnp.b...  3.91 us
  transfers between devices with their start and end apart: 29, of which 15 were waited for; matrix products, arithmetic and copies ran while one was open for 6% of the time, Pallas kernels for 11%

commit v1 on v0

--- a/solution.py
+++ b/solution.py
@@ -63,12 +63,12 @@
     )(tp_index, gain[None, :], *weights)
 
 
-def placed(slots, blocks):
+def placed(tp_index, blocks):
     n = len(blocks)
 
-    def body(slot_ref, *refs):
-        for i in range(n):
-            refs[n][slot_ref[i]] = refs[i][...]
+    def body(tp_ref, *refs):
+        for s in range(n):
+            refs[n][lax.rem(tp_ref[0] + (n - s), n)] = refs[s][...]
 
     return pl.pallas_call(
         body,
@@ -77,25 +77,26 @@
         out_specs=VMEM,
         compiler_params=VMEM_LIMIT,
         name="placed",
-    )(slots, *blocks)
-
-
-def fill(slot_ref, refs, all_ref):
-    for i, ref in enumerate(refs):
-        at = pl.multiple_of(slot_ref[i] * 64, 64)
-        all_ref[pl.ds(at, ref.shape[0]), :] = ref[...]
-
-
-def acted(slots, normed, blocks, gate_act=None, gates=None):
+    )(tp_index, *blocks)
+
+
+def fill(tp_ref, refs, all_ref):
+    rows = refs[0].shape[0]
+    for ref, ahead in zip(refs, (0, 3, 1, 2)):
+        at = pl.multiple_of(lax.rem(tp_ref[0] + ahead, 4) * rows, rows)
+        all_ref[pl.ds(at, rows), :] = ref[...]
+
+
+def acted(tp_index, normed, blocks, gate_act=None, gates=None):
     tokens, width = normed.shape
     n = len(blocks)
     units = 512
     step = tokens // 2
     last = gate_act is not None
 
-    def body(slot_ref, n_ref, *refs):
+    def body(tp_ref, n_ref, *refs):
         all_ref, out_ref = refs[-2:]
-        fill(slot_ref, refs[:n], all_ref)
+        fill(tp_ref, refs[:n], all_ref)
         low = lax.broadcasted_iota(jnp.int32, (step, 128), 1) < 64
 
         def one(i, _):
@@ -123,7 +124,7 @@
 
         lax.fori_loop(0, 2, one, 0)
 
-    args = [slots, normed, *blocks] + ([gate_act, gates] if last else [])
+    args = [tp_index, normed, *blocks] + ([gate_act, gates] if last else [])
     return pl.pallas_call(
         body,
         out_shape=[
@@ -164,30 +165,27 @@
 
 
 def gathered(name, own):
-    n_tp = lax.axis_size("tp")
-    tp = lax.axis_index("tp").astype(jnp.int32)
 
     def sent(block, by):
         return shifted(block, "tp", by)
 
     prev, after = sent(own, 1), sent(own, -1)
-    slots = [2 * tp, 2 * ((tp - 1) % n_tp), 2 * ((tp + 1) % n_tp), 2 * ((tp + 2) % n_tp)]
     if name in RELAYED:
         far = [sent(*((prev, 1) if RELAYED[name] > 0 else (after, -1)))]
     else:
         far = [sent(own, 2)]
-    return jnp.stack(slots), [own, prev, after] + far
-
-
-def mixed_away(slots, hidden, blocks):
+    return [own, prev, after] + far
+
+
+def mixed_away(tp_index, hidden, blocks):
     tokens, units = hidden.shape
     half = tokens // 2
     wide = blocks[0].shape[1]
     n = len(blocks)
 
-    def body(slot_ref, h_ref, *refs):
+    def body(tp_ref, h_ref, *refs):
         all_ref, away_ref = refs[n:]
-        fill(slot_ref, refs[:n], all_ref)
+        fill(tp_ref, refs[:n], all_ref)
 
         def one(i, _):
             at = pl.ds(pl.multiple_of(i * 256, 256), 256)
@@ -207,7 +205,7 @@
         out_specs=[VMEM] * 2,
         compiler_params=VMEM_LIMIT,
         name="mixed_away",
-    )(slots, hidden, *blocks)
+    )(tp_index, hidden, *blocks)
 
 
 def mixed_here(hidden, down, arrived, n_x):
@@ -247,7 +245,7 @@
     per = len(parts[0])
 
     def body(*refs):
-        out, total = refs[-2:]
+        outs, total = refs[len(flat) : -1], refs[-1]
         start = 0
         for c, wide in enumerate(widths):
             part = refs[c * per][...]
@@ -258,13 +256,16 @@
         for z in range(n_z):
             at = pl.ds(z * rows, rows)
             piece = jnp.concatenate([total[at, :half], total[at, half:]], axis=0)
-            out[z] = piece.astype(out.dtype)
-
-    return pl.pallas_call(
-        body,
-        out_shape=jax.ShapeDtypeStruct((n_z, 2 * rows, half), jnp.bfloat16),
+            outs[z][...] = piece.astype(outs[z].dtype)
+
+    return pl.pallas_call(
+        body,
+        out_shape=[
+            jax.ShapeDtypeStruct((2 * rows, half), jnp.bfloat16 if z else jnp.float32)
+            for z in range(n_z)
+        ],
         in_specs=[VMEM] * len(flat),
-        out_specs=VMEM,
+        out_specs=[VMEM] * n_z,
         scratch_shapes=[pltpu.VMEM((count, width), jnp.float32)],
         compiler_params=VMEM_LIMIT,
         name="folded",
@@ -272,37 +273,54 @@
 
 
 def finished(pieces):
-    n_z, rows, half = pieces.shape
-
-    def body(p_ref, out):
-        total = p_ref[0].astype(jnp.float32)
-        for z in range(1, n_z):
-            total = total + p_ref[z].astype(jnp.float32)
-        wide = jnp.concatenate([total[: rows // 2], total[rows // 2 :]], axis=1)
-        out[...] = wide.astype(jnp.bfloat16)
+    rows, half = pieces[0].shape
+
+    def body(*refs):
+        total = refs[0][...]
+        for r in refs[1:-1]:
+            total = total + r[...].astype(jnp.float32)
+        refs[-1][:, :half] = total[: rows // 2].astype(jnp.bfloat16)
+        refs[-1][:, half:] = total[rows // 2 :].astype(jnp.bfloat16)
 
     return pl.pallas_call(
         body,
         out_shape=jax.ShapeDtypeStruct((rows // 2, 2 * half), jnp.bfloat16),
-        in_specs=[VMEM],
+        in_specs=[VMEM] * len(pieces),
         out_specs=VMEM,
         compiler_params=VMEM_LIMIT,
         name="finished",
-    )(pieces)
+    )(*pieces)
+
+
+def side_by_side(parts):
+    rows = parts[0].shape[0]
+    widths = [p.shape[1] for p in parts]
+
+    def body(*refs):
+        for i, ref in enumerate(refs[:-1]):
+            refs[-1][:, pl.ds(sum(widths[:i]), widths[i])] = ref[...]
+
+    return pl.pallas_call(
+        body,
+        out_shape=jax.ShapeDtypeStruct((rows, sum(widths)), parts[0].dtype),
+        in_specs=[VMEM] * len(parts),
+        out_specs=VMEM,
+        compiler_params=VMEM_LIMIT,
+        name="side_by_side",
+    )(*parts)
 
 
 def local(tokens, norm_gain, gate_weight, up_weight, down_weight, expert_ids, expert_mix):
     tp = lax.axis_index("tp").astype(jnp.int32)
     tp_index = tp.reshape(1)
     n_tp = lax.axis_size("tp")
-    column_slots = jnp.stack([(tp - s) % n_tp for s in range(n_tp)])
 
     def handed(weights, scaled):
         blocks = prepare(tp_index, norm_gain, weights, scaled)
         arrived = [blocks[0]]
         for s in range(1, n_tp):
             arrived.append(shifted(blocks[s], "tp", s))
-        columns = placed(column_slots, arrived)
+        columns = placed(tp_index, arrived)
         columns = columns.reshape((-1,) + columns.shape[2:])
         return lax.all_to_all(columns, FS, split_axis=0, concat_axis=0, tiled=True)
 
@@ -321,7 +339,7 @@
     row = jnp.arange(count, dtype=jnp.int32)
     c_at = (row // (count // n_c) + lax.axis_index("fs_2")) % n_c
     x_at = (row // (count // n_c // n_x) + lax.axis_index("fs_1")) % n_x
-    z_at = (row // own_rows) % n_z
+    z_at = (row // own_rows + lax.axis_index("fs_0")) % n_z
     source = ((z_at * n_x + x_at) * n_c + c_at) * own_rows + row % own_rows
     pick = source[:, None] == row[None, :]
 
@@ -343,23 +361,24 @@
     )
     expert_gates = jnp.dot(pick.astype(jnp.float32), expert_gates, precision=lax.Precision.HIGHEST)
 
-    gate_all, gate_act = acted(gate_pieces[0], normed, gate_pieces[1])
-    up_all, hidden = acted(up_pieces[0], normed, up_pieces[1], gate_act, expert_gates)
+    gate_all, gate_act = acted(tp_index, normed, gate_pieces)
+    up_all, hidden = acted(tp_index, normed, up_pieces, gate_act, expert_gates)
     units = up_all.shape[0] // experts
 
     down_parts, summed = [], []
-    for slots, pieces in down_pieces:
-        down_c, away = mixed_away(slots, hidden, pieces)
+    for pieces in down_pieces:
+        down_c, away = mixed_away(tp_index, hidden, pieces)
         down_parts.append(down_c)
         away = shifted(away, "fs_2", 1)
         blocks = list(mixed_here(hidden, down_c, away, n_x))
         for s in range(1, n_x):
             blocks[s] = shifted(blocks[s], "fs_1", s)
         summed.append(blocks)
-    pieces = folded(summed, n_z)
-    pieces = lax.all_to_all(pieces, "fs_0", split_axis=0, concat_axis=0, tiled=True)
+    pieces = list(folded(summed, n_z))
+    for s in range(1, n_z):
+        pieces[s] = shifted(pieces[s], "fs_0", s)
     mixed = finished(pieces)[:, None, :]
-    down_all = jnp.concatenate(down_parts, axis=1)
+    down_all = side_by_side(down_parts)
 
     def as_served(a):
         return jnp.transpose(a.reshape(experts, units, width), (0, 2, 1))

time: 185 us -> 180 us (0.973)
  starting transfers between devices: 61.8 us -> 70.1 us
  Pallas kernels: 24.9 us -> 18.4 us
  waiting for transfers between devices: 80.8 us -> 77.3 us
    ppermute x26 -> x33, starting transfers between devices: 38.9 us -> 50.8 us  [shifted(): return lax.ppermute(array, axis, [(i, (i + by) % n) for i in range(n)])]
    all_to_all x1 -> x0, waiting for transfers between devices: 11.3 us -> none  [local(): lax.all_to_all(pieces, 'fs_0', split_axis=0, concat_axis=0, tiled=True)]
    ppermute x26 -> x33, waiting for transfers between devices: 43.6 us -> 50.1 us  [shifted(): return lax.ppermute(array, axis, [(i, (i + by) % n) for i in range(n)])]
    all_to_all x1 -> x0, starting transfers between devices: 3.56 us -> none  [local(): lax.all_to_all(pieces, 'fs_0', split_axis=0, concat_axis=0, tiled=True)]
    pallas_call x2, Pallas kernels: 8.1 us -> 5.04 us  [acted(): pl.pallas_call(body, out_shape=[jax.ShapeDtypeStruct((units, width), jnp....]
  transfers between devices with their start and end apart: 29 -> 35, of which waited for: 15 -> 18; matrix products, arithmetic and copies ran while one was open for 6% -> 5% of each run, Pallas kernels for 11% -> 8%
where the time goes in v1:
time: 180 us; the launch traced here: 179 us
  waiting for transfers between devices  77.3 us (43%)
  starting transfers between devices  70.1 us (39%)
  Pallas kernels  18.4 us (10%)
  matrix products  5.93 us (3%)
  other arithmetic  3.52 us (2%)
  local copies, waits for them, and re-layouts  3.12 us (2%)
    ppermute x33, starting transfers between devices, shifted(): return lax.ppermute(array, axis, [(i, (i + by) % n) for i in range(n)])  50.8 us
    ppermute x33, waiting for transfers between devices, shifted(): return lax.ppermute(array, axis, [(i, (i + by) % n) for i in range(n)])  50.1 us
    all_to_all x2, waiting for transfers between devices, handed(): return lax.all_to_all(columns, FS, split_axis=0, concat_axis=0, tiled=True)  27.2 us
    all_to_all x2, starting transfers between devices, handed(): return lax.all_to_all(columns, FS, split_axis=0, concat_axis=0, tiled=True)  19.3 us
    pallas_call x2, Pallas kernels, acted(): pl.pallas_call(body, out_shape=[jax.ShapeDtypeStruct((units, width), jnp....  5.04 us
    dot_general x1, matrix products, local(): jnp.dot(pick.astype(jnp.bfloat16), normed, preferred_element_type=jnp.flo...  4.76 us
  transfers between devices with their start and end apart: 35, of which 18 were waited for; matrix products, arithmetic and copies ran while one was open for 5% of the time, Pallas kernels for 8%

profile of v1, /device:TPU:1, one launch (start us, length us, event | category | flops | bytes accessed | tf_op | source)
XLA Modules:
  0.0 179.1 jit_solution(10855613757929309480)
XLA Ops:
  0.6 1.2 copy-done.1
  1.9 1.2 copy-done.2
  3.7 1.5 prepare.2
  5.3 2.2 %collective-permute-start = (bf16[16,2,32,128]{3,2,1,0:T(8,128)(2,1)S(1)}, bf16[16,2,32,128]{3,2,1,0:T(8,128)(2,1)S(1)}, u32[]{:S(2)}, u32[]{:S(2)}) collective-permute-start(bf16[16,2,32,128]{3,2,1,0:T(8,128)(2,1)S(1)} %get-tuple-element.41), channel_id=1, source_target_pairs={{0,1},{1,2},{2,3},{3,0},{4,5},{5,6},{6,7},{7,4},{8,9},{9,10},{10,1... | collective-permute-start | bytes 786440 | tf_op jit(solution)/shard_map/ppermute | solution.py:22
  7.5 2.6 %collective-permute-start.1 = (bf16[16,2,32,128]{3,2,1,0:T(8,128)(2,1)S(1)}, bf16[16,2,32,128]{3,2,1,0:T(8,128)(2,1)S(1)}, u32[]{:S(2)}, u32[]{:S(2)}) collective-permute-start(bf16[16,2,32,128]{3,2,1,0:T(8,128)(2,1)S(1)} %get-tuple-element.42), channel_id=1, source_target_pairs={{0,2},{1,3},{2,0},{3,1},{4,6},{5,7},{6,4},{7,5},{8,10},{9,11},{10,... | collective-permute-start | bytes 786440 | tf_op jit(solution)/shard_map/ppermute | solution.py:22
  10.1 1.1 collective-permute-start.2
  11.1 1.8 %collective-permute-done.refs_1_ = bf16[16,2,32,128]{3,2,1,0:T(8,128)(2,1)S(1)} collective-permute-done((bf16[16,2,32,128]{3,2,1,0:T(8,128)(2,1)S(1)}, bf16[16,2,32,128]{3,2,1,0:T(8,128)(2,1)S(1)}, u32[]{:S(2)}, u32[]{:S(2)}) %collective-permute-start) | collective-permute-done | bytes 262176 | tf_op jit(solution)/shard_map/ppermute | solution.py:22
  13.0 8.4 %collective-permute-done.1.refs_2_ = bf16[16,2,32,128]{3,2,1,0:T(8,128)(2,1)S(1)} collective-permute-done((bf16[16,2,32,128]{3,2,1,0:T(8,128)(2,1)S(1)}, bf16[16,2,32,128]{3,2,1,0:T(8,128)(2,1)S(1)}, u32[]{:S(2)}, u32[]{:S(2)}) %collective-permute-start.1) | collective-permute-done | bytes 262176 | tf_op jit(solution)/shard_map/ppermute | solution.py:22
  21.4 1.0 placed.2
  22.5 13.0 %all-to-all-start = ((bf16[64,2,32,128]{3,2,1,0:T(8,128)(2,1)}), bf16[64,2,32,128]{3,2,1,0:T(8,128)(2,1)S(1)}, u32[]{:S(2)}, u32[]{:S(2)}) async-start(bf16[64,2,32,128]{3,2,1,0:T(8,128)(2,1)} %bitcast.3), calls=%async_computation | async-start | bytes 2097152 | tf_op jit(solution)/shard_map/all_to_all | solution.py:325
  35.5 1.3 prepare.3
  36.8 1.0 collective-permute-start.9
  37.8 2.1 %collective-permute-start.10 = (bf16[16,1,32,128]{3,2,1,0:T(8,128)(2,1)S(1)}, bf16[16,1,32,128]{3,2,1,0:T(8,128)(2,1)S(1)}, u32[]{:S(2)}, u32[]{:S(2)}) collective-permute-start(bf16[16,1,32,128]{3,2,1,0:T(8,128)(2,1)S(1)} %get-tuple-element.52), channel_id=1, source_target_pairs={{0,2},{1,3},{2,0},{3,1},{4,6},{5,7},{6,4},{7,5},{8,10},{9,11},{10,... | collective-permute-start | bytes 393224 | tf_op jit(solution)/shard_map/ppermute | solution.py:22
  39.9 1.3 collective-permute-start.11
  41.3 1.4 collective-permute-done.9.refs_1_
  42.7 3.2 %collective-permute-done.10.refs_2_ = bf16[16,1,32,128]{3,2,1,0:T(8,128)(2,1)S(1)} collective-permute-done((bf16[16,1,32,128]{3,2,1,0:T(8,128)(2,1)S(1)}, bf16[16,1,32,128]{3,2,1,0:T(8,128)(2,1)S(1)}, u32[]{:S(2)}, u32[]{:S(2)}) %collective-permute-start.10) | collective-permute-done | bytes 131104 | tf_op jit(solution)/shard_map/ppermute | solution.py:22
  45.9 0.8 placed.3
  46.7 16.9 %all-to-all-done.x_ref = bf16[64,2,32,128]{3,2,1,0:T(8,128)(2,1)S(1)} async-done(((bf16[64,2,32,128]{3,2,1,0:T(8,128)(2,1)}), bf16[64,2,32,128]{3,2,1,0:T(8,128)(2,1)S(1)}, u32[]{:S(2)}, u32[]{:S(2)}) %all-to-all-start) | async-done | bytes 1048608 | tf_op jit(solution)/shard_map/all_to_all | solution.py:325
  63.7 6.3 %all-to-all-start.1 = ((bf16[64,1,32,128]{3,2,1,0:T(8,128)(2,1)}), bf16[64,1,32,128]{3,2,1,0:T(8,128)(2,1)S(1)}, u32[]{:S(2)}, u32[]{:S(2)}) async-start(bf16[64,1,32,128]{3,2,1,0:T(8,128)(2,1)} %bitcast.10), calls=%async_computation.1 | async-start | bytes 1048576 | tf_op jit(solution)/shard_map/all_to_all | solution.py:325
  69.9 2.5 %convert_reduce_fusion = f32[768]{0:T(1024)S(1)} fusion(bf16[768,1,2048]{2,0,1:T(8,128)(2,1)} %param.7), kind=kLoop, calls=%fused_computation | loop fusion | flops 3144960 | bytes 3148800 | tf_op jit(solution)/shard_map/reduce_sum | solution.py:347
  72.5 1.1 turned.2
  73.6 1.0 collective-permute-start.3
  74.7 1.7 collective-permute-start.7
  76.4 1.0 fusion.3
  77.3 10.3 %all-to-all-done.1.x_ref = bf16[64,1,32,128]{3,2,1,0:T(8,128)(2,1)S(1)} async-done(((bf16[64,1,32,128]{3,2,1,0:T(8,128)(2,1)}), bf16[64,1,32,128]{3,2,1,0:T(8,128)(2,1)S(1)}, u32[]{:S(2)}, u32[]{:S(2)}) %all-to-all-start.1) | async-done | bytes 524320 | tf_op jit(solution)/shard_map/all_to_all | solution.py:325
  88.2 1.0 collective-permute-start.12
  89.3 1.7 collective-permute-start.4
  91.0 0.8 collective-permute-start.5
  91.7 2.0 %collective-permute-start.8 = (bf16[128,2048]{1,0:T(8,128)(2,1)S(1)}, bf16[128,2048]{1,0:T(8,128)(2,1)S(1)}, u32[]{:S(2)}, u32[]{:S(2)}) collective-permute-start(bf16[128,2048]{1,0:T(8,128)(2,1)S(1)} %collective-permute-done.7.refs_2_), channel_id=1, source_target_pairs={{0,3},{1,0},{2,1},{3,2},{4,7},{5,4},{6,5},{7,6},{8,11},{9,8},{10,9... | collective-permute-start | bytes 1572872 | tf_op jit(solution)/shard_map/ppermute | solution.py:22
  93.7 4.8 %convolution_convert_fusion.n_ref = bf16[768,2048]{1,0:T(8,128)(2,1)S(1)} fusion(bf16[768,1,2048]{2,0,1:T(8,128)(2,1)} %param.7, f32[768]{0:T(1024)S(1)} %add_rsqrt_fusion, f32[768]{0:T(1024)S(1)} %broadcast_multiply_fusion, s32[768]{0:T(1024)S(1)} %fusion.26), kind=kOutput, calls=%fused_computation.7 | convolution fusion | flops 2424373248 | bytes 6300672 | tf_op jit(solution)/shard_map/dot_general | solution.py:351
  98.5 1.5 collective-permute-start.13
  100.0 2.1 %collective-permute-done.4.refs_2_ = bf16[128,2048]{1,0:T(8,128)(2,1)S(1)} collective-permute-done((bf16[128,2048]{1,0:T(8,128)(2,1)S(1)}, bf16[128,2048]{1,0:T(8,128)(2,1)S(1)}, u32[]{:S(2)}, u32[]{:S(2)}) %collective-permute-start.4) | collective-permute-done | bytes 524320 | tf_op jit(solution)/shard_map/ppermute | solution.py:22
  102.1 2.1 %collective-permute-start.14 = (bf16[128,1024]{1,0:T(8,128)(2,1)S(1)}, bf16[128,1024]{1,0:T(8,128)(2,1)S(1)}, u32[]{:S(2)}, u32[]{:S(2)}) collective-permute-start(bf16[128,1024]{1,0:T(8,128)(2,1)S(1)} %get-tuple-element.54.refs_0_), channel_id=1, source_target_pairs={{0,2},{1,3},{2,0},{3,1},{4,6},{5,7},{6,4},{7,5},{8,10},{9,11},{10,... | collective-permute-start | bytes 786440 | tf_op jit(solution)/shard_map/ppermute | solution.py:22
  104.2 4.0 %collective-permute-done.6.refs_1_ = bf16[128,2048]{1,0:T(8,128)(2,1)S(1)} collective-permute-done((bf16[128,2048]{1,0:T(8,128)(2,1)S(1)}, bf16[128,2048]{1,0:T(8,128)(2,1)S(1)}, u32[]{:S(2)}, u32[]{:S(2)}) %collective-permute-start.6) | collective-permute-done | bytes 524320 | tf_op jit(solution)/shard_map/ppermute | solution.py:22
  108.2 11.2 %collective-permute-done.5.refs_3_ = bf16[128,2048]{1,0:T(8,128)(2,1)S(1)} collective-permute-done((bf16[128,2048]{1,0:T(8,128)(2,1)S(1)}, bf16[128,2048]{1,0:T(8,128)(2,1)S(1)}, u32[]{:S(2)}, u32[]{:S(2)}) %collective-permute-start.5) | collective-permute-done | bytes 524320 | tf_op jit(solution)/shard_map/ppermute | solution.py:22
  120.1 0.9 collective-permute-start.17
  121.0 1.2 fusion.8.refs_5_
  122.2 2.5 %acted.2 = (bf16[512,2048]{1,0:T(8,128)(2,1)}, f32[768,512]{1,0:T(8,128)S(1)}) custom-call(s32[1]{0:T(128)} %bitcast.tp_ref, bf16[768,2048]{1,0:T(8,128)(2,1)S(1)} %convolution_convert_fusion.n_ref, bf16[128,2048]{1,0:T(8,128)(2,1)S(1)} %get-tuple-element.44.refs_0_, bf16[128,2048]{1,0:T(8,128)(2,1)S(1)} %collective-permute-done.3.refs_1_, ...), custom_call_target="tpu_custom_call" | custom-call | tf_op jit(solution)/shard_map/acted/pallas_call | solution.py:128
  124.6 2.6 %acted.3 = (bf16[512,2048]{1,0:T(8,128)(2,1)}, bf16[768,512]{1,0:T(8,128)(2,1)S(1)}) custom-call(s32[1]{0:T(128)} %bitcast.tp_ref, bf16[768,2048]{1,0:T(8,128)(2,1)S(1)} %convolution_convert_fusion.n_ref, bf16[128,2048]{1,0:T(8,128)(2,1)S(1)} %get-tuple-element.46.refs_0_, bf16[128,2048]{1,0:T(8,128)(2,1)S(1)} %collective-permute-done.6.refs_1_, ...), custom_call_target="tpu_custom_call" | custom-call | tf_op jit(solution)/shard_map/acted/pallas_call | solution.py:128
  127.2 1.2 mixed_away.2
  128.4 7.4 %collective-permute-start.18 = (bf16[384,1024]{1,0:T(8,128)(2,1)S(1)}, bf16[384,1024]{1,0:T(8,128)(2,1)S(1)}, u32[]{:S(2)}, u32[]{:S(2)}) collective-permute-start(bf16[384,1024]{1,0:T(8,128)(2,1)S(1)} %get-tuple-element.58), channel_id=1, source_target_pairs={{0,4},{4,0},{1,5},{5,1},{2,6},{6,2},{3,7},{7,3},{8,12},{12,8},{9,1... | collective-permute-start | bytes 2359304 | tf_op jit(solution)/shard_map/ppermute | solution.py:22
  135.8 0.9 collective-permute-done.17.refs_3_
  136.7 1.2 mixed_away.3
  137.9 1.6 collective-permute-start.22
  139.5 1.1 mixed_here.2
  140.6 1.2 collective-permute-start.19
  141.7 1.2 collective-permute-start.20
  142.9 1.6 collective-permute-start.21
  144.5 1.1 mixed_here.3
  145.7 1.6 collective-permute-start.24
  147.4 1.4 collective-permute-done.19.refs_1_
  149.0 3.2 %collective-permute-done.20.refs_2_ = bf16[96,1024]{1,0:T(8,128)(2,1)S(1)} collective-permute-done((bf16[96,1024]{1,0:T(8,128)(2,1)S(1)}, bf16[96,1024]{1,0:T(8,128)(2,1)S(1)}, u32[]{:S(2)}, u32[]{:S(2)}) %collective-permute-start.20) | collective-permute-done | bytes 196640 | tf_op jit(solution)/shard_map/ppermute | solution.py:22
  152.1 0.7 collective-permute-done.21.refs_3_
  152.9 4.5 %collective-permute-done.23.refs_5_ = bf16[96,1024]{1,0:T(8,128)(2,1)S(1)} collective-permute-done((bf16[96,1024]{1,0:T(8,128)(2,1)S(1)}, bf16[96,1024]{1,0:T(8,128)(2,1)S(1)}, u32[]{:S(2)}, u32[]{:S(2)}) %collective-permute-start.23) | collective-permute-done | bytes 196640 | tf_op jit(solution)/shard_map/ppermute | solution.py:22
  157.4 3.2 %collective-permute-done.24.refs_6_ = bf16[96,1024]{1,0:T(8,128)(2,1)S(1)} collective-permute-done((bf16[96,1024]{1,0:T(8,128)(2,1)S(1)}, bf16[96,1024]{1,0:T(8,128)(2,1)S(1)}, u32[]{:S(2)}, u32[]{:S(2)}) %collective-permute-start.24) | collective-permute-done | bytes 196640 | tf_op jit(solution)/shard_map/ppermute | solution.py:22
  161.6 0.8 collective-permute-start.26
  162.4 1.0 collective-permute-start.27
  163.4 2.8 %collective-permute-start.28 = (bf16[24,1024]{1,0:T(8,128)(2,1)S(1)}, bf16[24,1024]{1,0:T(8,128)(2,1)S(1)}, u32[]{:S(2)}, u32[]{:S(2)}) collective-permute-start(bf16[24,1024]{1,0:T(8,128)(2,1)S(1)} %get-tuple-element.71), channel_id=1, source_target_pairs={{0,96},{32,128},{64,160},{96,192},{128,224},{160,0},{192,32},{224,... | collective-permute-start | bytes 147464 | tf_op jit(solution)/shard_map/ppermute | solution.py:22
  166.1 1.7 collective-permute-start.29
  167.8 3.3 %collective-permute-start.30 = (bf16[24,1024]{1,0:T(8,128)(2,1)S(1)}, bf16[24,1024]{1,0:T(8,128)(2,1)S(1)}, u32[]{:S(2)}, u32[]{:S(2)}) collective-permute-start(bf16[24,1024]{1,0:T(8,128)(2,1)S(1)} %get-tuple-element.73), channel_id=1, source_target_pairs={{0,160},{32,192},{64,224},{96,0},{128,32},{160,64},{192,96},{224,1... | collective-permute-start | bytes 147464 | tf_op jit(solution)/shard_map/ppermute | solution.py:22
  171.2 2.0 %collective-permute-start.31 = (bf16[24,1024]{1,0:T(8,128)(2,1)S(1)}, bf16[24,1024]{1,0:T(8,128)(2,1)S(1)}, u32[]{:S(2)}, u32[]{:S(2)}) collective-permute-start(bf16[24,1024]{1,0:T(8,128)(2,1)S(1)} %get-tuple-element.74), channel_id=1, source_target_pairs={{0,192},{32,224},{64,0},{96,32},{128,64},{160,96},{192,128},{224,1... | collective-permute-start | bytes 147464 | tf_op jit(solution)/shard_map/ppermute | solution.py:22
  173.8 1.5 side_by_side.1
  175.3 2.0 %collective-permute-done.31.refs_6_ = bf16[24,1024]{1,0:T(8,128)(2,1)S(1)} collective-permute-done((bf16[24,1024]{1,0:T(8,128)(2,1)S(1)}, bf16[24,1024]{1,0:T(8,128)(2,1)S(1)}, u32[]{:S(2)}, u32[]{:S(2)}) %collective-permute-start.31) | collective-permute-done | bytes 49184 | tf_op jit(solution)/shard_map/ppermute | solution.py:22
  177.3 1.2 collective-permute-done.32.refs_7_
  (45 shorter events, 4.7 us)
Async XLA Ops:
  0.6 1.2 copy-start.1
  1.9 1.2 copy-start.2
  3.1 0.7 copy-start.3
  3.7 31.7 %copy-start = (f32[8,32,1024]{2,1,0:T(8,128)S(1)}, f32[8,32,1024]{2,1,0:T(8,128)}, u32[]{:S(2)}) copy-start(f32[8,32,1024]{2,1,0:T(8,128)} %refs_0_.3) | copy-start | bytes 3145732
  3.7 31.8 %copy-start.4 = (f32[32]{0:T(128)S(1)}, f32[32]{0:T(128)}, u32[]{:S(2)}) copy-start(f32[32]{0:T(128)} %param.8) | copy-start | bytes 388
  5.3 7.7 %collective-permute-start = (bf16[16,2,32,128]{3,2,1,0:T(8,128)(2,1)S(1)}, bf16[16,2,32,128]{3,2,1,0:T(8,128)(2,1)S(1)}, u32[]{:S(2)}, u32[]{:S(2)}) collective-permute-start(bf16[16,2,32,128]{3,2,1,0:T(8,128)(2,1)S(1)} %get-tuple-element.41), channel_id=1, source_target_pairs={{0,1},{1,2},{2,3},{3,0},{4,5},{5,6},{6,7},{7,4},{8,9},{9,10},{10,1... | collective-permute-start | bytes 786440 | tf_op jit(solution)/shard_map/ppermute | solution.py:22
  7.5 14.0 %collective-permute-start.1 = (bf16[16,2,32,128]{3,2,1,0:T(8,128)(2,1)S(1)}, bf16[16,2,32,128]{3,2,1,0:T(8,128)(2,1)S(1)}, u32[]{:S(2)}, u32[]{:S(2)}) collective-permute-start(bf16[16,2,32,128]{3,2,1,0:T(8,128)(2,1)S(1)} %get-tuple-element.42), channel_id=1, source_target_pairs={{0,2},{1,3},{2,0},{3,1},{4,6},{5,7},{6,4},{7,5},{8,10},{9,11},{10,... | collective-permute-start | bytes 786440 | tf_op jit(solution)/shard_map/ppermute | solution.py:22
  10.1 11.3 %collective-permute-start.2 = (bf16[16,2,32,128]{3,2,1,0:T(8,128)(2,1)S(1)}, bf16[16,2,32,128]{3,2,1,0:T(8,128)(2,1)S(1)}, u32[]{:S(2)}, u32[]{:S(2)}) collective-permute-start(bf16[16,2,32,128]{3,2,1,0:T(8,128)(2,1)S(1)} %get-tuple-element.43), channel_id=1, source_target_pairs={{0,3},{1,0},{2,1},{3,2},{4,7},{5,4},{6,5},{7,6},{8,11},{9,8},{10,9... | collective-permute-start | bytes 786440 | tf_op jit(solution)/shard_map/ppermute | solution.py:22
  22.5 41.2 %all-to-all-start = ((bf16[64,2,32,128]{3,2,1,0:T(8,128)(2,1)}), bf16[64,2,32,128]{3,2,1,0:T(8,128)(2,1)S(1)}, u32[]{:S(2)}, u32[]{:S(2)}) async-start(bf16[64,2,32,128]{3,2,1,0:T(8,128)(2,1)} %bitcast.3), calls=%async_computation | async-start | bytes 2097152 | tf_op jit(solution)/shard_map/all_to_all | solution.py:325
  36.8 5.9 %collective-permute-start.9 = (bf16[16,1,32,128]{3,2,1,0:T(8,128)(2,1)S(1)}, bf16[16,1,32,128]{3,2,1,0:T(8,128)(2,1)S(1)}, u32[]{:S(2)}, u32[]{:S(2)}) collective-permute-start(bf16[16,1,32,128]{3,2,1,0:T(8,128)(2,1)S(1)} %get-tuple-element.51), channel_id=1, source_target_pairs={{0,1},{1,2},{2,3},{3,0},{4,5},{5,6},{6,7},{7,4},{8,9},{9,10},{10,1... | collective-permute-start | bytes 393224 | tf_op jit(solution)/shard_map/ppermute | solution.py:22
  37.8 8.1 %collective-permute-start.10 = (bf16[16,1,32,128]{3,2,1,0:T(8,128)(2,1)S(1)}, bf16[16,1,32,128]{3,2,1,0:T(8,128)(2,1)S(1)}, u32[]{:S(2)}, u32[]{:S(2)}) collective-permute-start(bf16[16,1,32,128]{3,2,1,0:T(8,128)(2,1)S(1)} %get-tuple-element.52), channel_id=1, source_target_pairs={{0,2},{1,3},{2,0},{3,1},{4,6},{5,7},{6,4},{7,5},{8,10},{9,11},{10,... | collective-permute-start | bytes 393224 | tf_op jit(solution)/shard_map/ppermute | solution.py:22
  39.9 5.9 %collective-permute-start.11 = (bf16[16,1,32,128]{3,2,1,0:T(8,128)(2,1)S(1)}, bf16[16,1,32,128]{3,2,1,0:T(8,128)(2,1)S(1)}, u32[]{:S(2)}, u32[]{:S(2)}) collective-permute-start(bf16[16,1,32,128]{3,2,1,0:T(8,128)(2,1)S(1)} %get-tuple-element.53), channel_id=1, source_target_pairs={{0,3},{1,0},{2,1},{3,2},{4,7},{5,4},{6,5},{7,6},{8,11},{9,8},{10,9... | collective-permute-start | bytes 393224 | tf_op jit(solution)/shard_map/ppermute | solution.py:22
  63.7 24.0 %all-to-all-start.1 = ((bf16[64,1,32,128]{3,2,1,0:T(8,128)(2,1)}), bf16[64,1,32,128]{3,2,1,0:T(8,128)(2,1)S(1)}, u32[]{:S(2)}, u32[]{:S(2)}) async-start(bf16[64,1,32,128]{3,2,1,0:T(8,128)(2,1)} %bitcast.10), calls=%async_computation.1 | async-start | bytes 1048576 | tf_op jit(solution)/shard_map/all_to_all | solution.py:325
  69.9 6.4 %copy-start.5 = (bf16[768,1,2048]{2,0,1:T(8,128)(2,1)S(1)}, bf16[768,1,2048]{2,0,1:T(8,128)(2,1)}, u32[]{:S(2)}) copy-start(bf16[768,1,2048]{2,0,1:T(8,128)(2,1)} %param.7) | copy-start | bytes 9437188
  73.6 17.4 %collective-permute-start.3 = (bf16[128,2048]{1,0:T(8,128)(2,1)S(1)}, bf16[128,2048]{1,0:T(8,128)(2,1)S(1)}, u32[]{:S(2)}, u32[]{:S(2)}) collective-permute-start(bf16[128,2048]{1,0:T(8,128)(2,1)S(1)} %get-tuple-element.44.refs_0_), channel_id=1, source_target_pairs={{0,1},{1,2},{2,3},{3,0},{4,5},{5,6},{6,7},{7,4},{8,9},{9,10},{10,1... | collective-permute-start | bytes 1572872 | tf_op jit(solution)/shard_map/ppermute | solution.py:22
  74.7 17.1 %collective-permute-start.7 = (bf16[128,2048]{1,0:T(8,128)(2,1)S(1)}, bf16[128,2048]{1,0:T(8,128)(2,1)S(1)}, u32[]{:S(2)}, u32[]{:S(2)}) collective-permute-start(bf16[128,2048]{1,0:T(8,128)(2,1)S(1)} %get-tuple-element.46.refs_0_), channel_id=1, source_target_pairs={{0,3},{1,0},{2,1},{3,2},{4,7},{5,4},{6,5},{7,6},{8,11},{9,8},{10,9... | collective-permute-start | bytes 1572872 | tf_op jit(solution)/shard_map/ppermute | solution.py:22
  88.2 16.0 %copy-start.6 = (f32[768,1,2]{0,2,1:T(2,128)S(1)}, f32[768,1,2]{0,2,1:T(2,128)}, u32[]{:S(2)}) copy-start(f32[768,1,2]{0,2,1:T(2,128)} %param.13) | copy-start | bytes 18436
  88.2 16.0 %copy-start.7 = (s32[768,1,2]{0,2,1:T(2,128)S(1)}, s32[768,1,2]{0,2,1:T(2,128)}, u32[]{:S(2)}) copy-start(s32[768,1,2]{0,2,1:T(2,128)} %param.12) | copy-start | bytes 18436
  88.2 10.3 %collective-permute-start.12 = (bf16[128,1024]{1,0:T(8,128)(2,1)S(1)}, bf16[128,1024]{1,0:T(8,128)(2,1)S(1)}, u32[]{:S(2)}, u32[]{:S(2)}) collective-permute-start(bf16[128,1024]{1,0:T(8,128)(2,1)S(1)} %get-tuple-element.54.refs_0_), channel_id=1, source_target_pairs={{0,1},{1,2},{2,3},{3,0},{4,5},{5,6},{6,7},{7,4},{8,9},{9,10},{10,1... | collective-permute-start | bytes 786440 | tf_op jit(solution)/shard_map/ppermute | solution.py:22
  89.3 12.8 %collective-permute-start.4 = (bf16[128,2048]{1,0:T(8,128)(2,1)S(1)}, bf16[128,2048]{1,0:T(8,128)(2,1)S(1)}, u32[]{:S(2)}, u32[]{:S(2)}) collective-permute-start(bf16[128,2048]{1,0:T(8,128)(2,1)S(1)} %get-tuple-element.44.refs_0_), channel_id=1, source_target_pairs={{0,3},{1,0},{2,1},{3,2},{4,7},{5,4},{6,5},{7,6},{8,11},{9,8},{10,9... | collective-permute-start | bytes 1572872 | tf_op jit(solution)/shard_map/ppermute | solution.py:22
  91.0 17.2 %collective-permute-start.6 = (bf16[128,2048]{1,0:T(8,128)(2,1)S(1)}, bf16[128,2048]{1,0:T(8,128)(2,1)S(1)}, u32[]{:S(2)}, u32[]{:S(2)}) collective-permute-start(bf16[128,2048]{1,0:T(8,128)(2,1)S(1)} %get-tuple-element.46.refs_0_), channel_id=1, source_target_pairs={{0,1},{1,2},{2,3},{3,0},{4,5},{5,6},{6,7},{7,4},{8,9},{9,10},{10,1... | collective-permute-start | bytes 1572872 | tf_op jit(solution)/shard_map/ppermute | solution.py:22
  91.0 28.5 %collective-permute-start.5 = (bf16[128,2048]{1,0:T(8,128)(2,1)S(1)}, bf16[128,2048]{1,0:T(8,128)(2,1)S(1)}, u32[]{:S(2)}, u32[]{:S(2)}) collective-permute-start(bf16[128,2048]{1,0:T(8,128)(2,1)S(1)} %collective-permute-done.3.refs_1_), channel_id=1, source_target_pairs={{0,1},{1,2},{2,3},{3,0},{4,5},{5,6},{6,7},{7,4},{8,9},{9,10},{10,1... | collective-permute-start | bytes 1572872 | tf_op jit(solution)/shard_map/ppermute | solution.py:22
  91.7 28.4 %collective-permute-start.8 = (bf16[128,2048]{1,0:T(8,128)(2,1)S(1)}, bf16[128,2048]{1,0:T(8,128)(2,1)S(1)}, u32[]{:S(2)}, u32[]{:S(2)}) collective-permute-start(bf16[128,2048]{1,0:T(8,128)(2,1)S(1)} %collective-permute-done.7.refs_2_), channel_id=1, source_target_pairs={{0,3},{1,0},{2,1},{3,2},{4,7},{5,4},{6,5},{7,6},{8,11},{9,8},{10,9... | collective-permute-start | bytes 1572872 | tf_op jit(solution)/shard_map/ppermute | solution.py:22
  98.5 28.7 %collective-permute-start.13 = (bf16[128,1024]{1,0:T(8,128)(2,1)S(1)}, bf16[128,1024]{1,0:T(8,128)(2,1)S(1)}, u32[]{:S(2)}, u32[]{:S(2)}) collective-permute-start(bf16[128,1024]{1,0:T(8,128)(2,1)S(1)} %get-tuple-element.54.refs_0_), channel_id=1, source_target_pairs={{0,3},{1,0},{2,1},{3,2},{4,7},{5,4},{6,5},{7,6},{8,11},{9,8},{10,9... | collective-permute-start | bytes 786440 | tf_op jit(solution)/shard_map/ppermute | solution.py:22
  102.1 25.1 %collective-permute-start.14 = (bf16[128,1024]{1,0:T(8,128)(2,1)S(1)}, bf16[128,1024]{1,0:T(8,128)(2,1)S(1)}, u32[]{:S(2)}, u32[]{:S(2)}) collective-permute-start(bf16[128,1024]{1,0:T(8,128)(2,1)S(1)} %get-tuple-element.54.refs_0_), channel_id=1, source_target_pairs={{0,2},{1,3},{2,0},{3,1},{4,6},{5,7},{6,4},{7,5},{8,10},{9,11},{10,... | collective-permute-start | bytes 786440 | tf_op jit(solution)/shard_map/ppermute | solution.py:22
  108.2 27.6 %collective-permute-start.15 = (bf16[128,1024]{1,0:T(8,128)(2,1)S(1)}, bf16[128,1024]{1,0:T(8,128)(2,1)S(1)}, u32[]{:S(2)}, u32[]{:S(2)}) collective-permute-start(bf16[128,1024]{1,0:T(8,128)(2,1)S(1)} %get-tuple-element.56.refs_0_), channel_id=1, source_target_pairs={{0,1},{1,2},{2,3},{3,0},{4,5},{5,6},{6,7},{7,4},{8,9},{9,10},{10,1... | collective-permute-start | bytes 786440 | tf_op jit(solution)/shard_map/ppermute | solution.py:22
  119.4 16.4 %collective-permute-start.16 = (bf16[128,1024]{1,0:T(8,128)(2,1)S(1)}, bf16[128,1024]{1,0:T(8,128)(2,1)S(1)}, u32[]{:S(2)}, u32[]{:S(2)}) collective-permute-start(bf16[128,1024]{1,0:T(8,128)(2,1)S(1)} %get-tuple-element.56.refs_0_), channel_id=1, source_target_pairs={{0,3},{1,0},{2,1},{3,2},{4,7},{5,4},{6,5},{7,6},{8,11},{9,8},{10,9... | collective-permute-start | bytes 786440 | tf_op jit(solution)/shard_map/ppermute | solution.py:22
  120.1 16.6 %collective-permute-start.17 = (bf16[128,1024]{1,0:T(8,128)(2,1)S(1)}, bf16[128,1024]{1,0:T(8,128)(2,1)S(1)}, u32[]{:S(2)}, u32[]{:S(2)}) collective-permute-start(bf16[128,1024]{1,0:T(8,128)(2,1)S(1)} %get-tuple-element.56.refs_0_), channel_id=1, source_target_pairs={{0,2},{1,3},{2,0},{3,1},{4,6},{5,7},{6,4},{7,5},{8,10},{9,11},{10,... | collective-permute-start | bytes 786440 | tf_op jit(solution)/shard_map/ppermute | solution.py:22
  128.4 11.1 %collective-permute-start.18 = (bf16[384,1024]{1,0:T(8,128)(2,1)S(1)}, bf16[384,1024]{1,0:T(8,128)(2,1)S(1)}, u32[]{:S(2)}, u32[]{:S(2)}) collective-permute-start(bf16[384,1024]{1,0:T(8,128)(2,1)S(1)} %get-tuple-element.58), channel_id=1, source_target_pairs={{0,4},{4,0},{1,5},{5,1},{2,6},{6,2},{3,7},{7,3},{8,12},{12,8},{9,1... | collective-permute-start | bytes 2359304 | tf_op jit(solution)/shard_map/ppermute | solution.py:22
  137.9 6.6 %collective-permute-start.22 = (bf16[384,1024]{1,0:T(8,128)(2,1)S(1)}, bf16[384,1024]{1,0:T(8,128)(2,1)S(1)}, u32[]{:S(2)}, u32[]{:S(2)}) collective-permute-start(bf16[384,1024]{1,0:T(8,128)(2,1)S(1)} %get-tuple-element.63), channel_id=1, source_target_pairs={{0,4},{4,0},{1,5},{5,1},{2,6},{6,2},{3,7},{7,3},{8,12},{12,8},{9,1... | collective-permute-start | bytes 2359304 | tf_op jit(solution)/shard_map/ppermute | solution.py:22
  140.6 8.1 %collective-permute-start.19 = (bf16[96,1024]{1,0:T(8,128)(2,1)S(1)}, bf16[96,1024]{1,0:T(8,128)(2,1)S(1)}, u32[]{:S(2)}, u32[]{:S(2)}) collective-permute-start(bf16[96,1024]{1,0:T(8,128)(2,1)S(1)} %get-tuple-element.60), channel_id=1, source_target_pairs={{0,8},{8,16},{16,24},{24,0},{1,9},{9,17},{17,25},{25,1},{2,10},{10... | collective-permute-start | bytes 589832 | tf_op jit(solution)/shard_map/ppermute | solution.py:22
  141.7 10.4 %collective-permute-start.20 = (bf16[96,1024]{1,0:T(8,128)(2,1)S(1)}, bf16[96,1024]{1,0:T(8,128)(2,1)S(1)}, u32[]{:S(2)}, u32[]{:S(2)}) collective-permute-start(bf16[96,1024]{1,0:T(8,128)(2,1)S(1)} %get-tuple-element.61), channel_id=1, source_target_pairs={{0,16},{8,24},{16,0},{24,8},{1,17},{9,25},{17,1},{25,9},{2,18},{10... | collective-permute-start | bytes 589832 | tf_op jit(solution)/shard_map/ppermute | solution.py:22
  142.9 9.9 %collective-permute-start.21 = (bf16[96,1024]{1,0:T(8,128)(2,1)S(1)}, bf16[96,1024]{1,0:T(8,128)(2,1)S(1)}, u32[]{:S(2)}, u32[]{:S(2)}) collective-permute-start(bf16[96,1024]{1,0:T(8,128)(2,1)S(1)} %get-tuple-element.62), channel_id=1, source_target_pairs={{0,24},{8,0},{16,8},{24,16},{1,25},{9,1},{17,9},{25,17},{2,26},{10... | collective-permute-start | bytes 589832 | tf_op jit(solution)/shard_map/ppermute | solution.py:22
  145.6 11.7 %collective-permute-start.23 = (bf16[96,1024]{1,0:T(8,128)(2,1)S(1)}, bf16[96,1024]{1,0:T(8,128)(2,1)S(1)}, u32[]{:S(2)}, u32[]{:S(2)}) collective-permute-start(bf16[96,1024]{1,0:T(8,128)(2,1)S(1)} %get-tuple-element.65), channel_id=1, source_target_pairs={{0,8},{8,16},{16,24},{24,0},{1,9},{9,17},{17,25},{25,1},{2,10},{10... | collective-permute-start | bytes 589832 | tf_op jit(solution)/shard_map/ppermute | solution.py:22
  145.7 14.9 %collective-permute-start.24 = (bf16[96,1024]{1,0:T(8,128)(2,1)S(1)}, bf16[96,1024]{1,0:T(8,128)(2,1)S(1)}, u32[]{:S(2)}, u32[]{:S(2)}) collective-permute-start(bf16[96,1024]{1,0:T(8,128)(2,1)S(1)} %get-tuple-element.66), channel_id=1, source_target_pairs={{0,16},{8,24},{16,0},{24,8},{1,17},{9,25},{17,1},{25,9},{2,18},{10... | collective-permute-start | bytes 589832 | tf_op jit(solution)/shard_map/ppermute | solution.py:22
  148.7 12.6 %collective-permute-start.25 = (bf16[96,1024]{1,0:T(8,128)(2,1)S(1)}, bf16[96,1024]{1,0:T(8,128)(2,1)S(1)}, u32[]{:S(2)}, u32[]{:S(2)}) collective-permute-start(bf16[96,1024]{1,0:T(8,128)(2,1)S(1)} %get-tuple-element.67), channel_id=1, source_target_pairs={{0,24},{8,0},{16,8},{24,16},{1,25},{9,1},{17,9},{25,17},{2,26},{10... | collective-permute-start | bytes 589832 | tf_op jit(solution)/shard_map/ppermute | solution.py:22
  161.6 9.6 %collective-permute-start.26 = (bf16[24,1024]{1,0:T(8,128)(2,1)S(1)}, bf16[24,1024]{1,0:T(8,128)(2,1)S(1)}, u32[]{:S(2)}, u32[]{:S(2)}) collective-permute-start(bf16[24,1024]{1,0:T(8,128)(2,1)S(1)} %get-tuple-element.69), channel_id=1, source_target_pairs={{0,32},{32,64},{64,96},{96,128},{128,160},{160,192},{192,224},{224... | collective-permute-start | bytes 147464 | tf_op jit(solution)/shard_map/ppermute | solution.py:22
  162.4 10.8 %collective-permute-start.27 = (bf16[24,1024]{1,0:T(8,128)(2,1)S(1)}, bf16[24,1024]{1,0:T(8,128)(2,1)S(1)}, u32[]{:S(2)}, u32[]{:S(2)}) collective-permute-start(bf16[24,1024]{1,0:T(8,128)(2,1)S(1)} %get-tuple-element.70), channel_id=1, source_target_pairs={{0,64},{32,96},{64,128},{96,160},{128,192},{160,224},{192,0},{224,... | collective-permute-start | bytes 147464 | tf_op jit(solution)/shard_map/ppermute | solution.py:22
  163.4 11.9 %collective-permute-start.28 = (bf16[24,1024]{1,0:T(8,128)(2,1)S(1)}, bf16[24,1024]{1,0:T(8,128)(2,1)S(1)}, u32[]{:S(2)}, u32[]{:S(2)}) collective-permute-start(bf16[24,1024]{1,0:T(8,128)(2,1)S(1)} %get-tuple-element.71), channel_id=1, source_target_pairs={{0,96},{32,128},{64,160},{96,192},{128,224},{160,0},{192,32},{224,... | collective-permute-start | bytes 147464 | tf_op jit(solution)/shard_map/ppermute | solution.py:22
  166.1 9.1 %collective-permute-start.29 = (bf16[24,1024]{1,0:T(8,128)(2,1)S(1)}, bf16[24,1024]{1,0:T(8,128)(2,1)S(1)}, u32[]{:S(2)}, u32[]{:S(2)}) collective-permute-start(bf16[24,1024]{1,0:T(8,128)(2,1)S(1)} %get-tuple-element.72), channel_id=1, source_target_pairs={{0,128},{32,160},{64,192},{96,224},{128,0},{160,32},{192,64},{224,... | collective-permute-start | bytes 147464 | tf_op jit(solution)/shard_map/ppermute | solution.py:22
  167.8 7.4 %collective-permute-start.30 = (bf16[24,1024]{1,0:T(8,128)(2,1)S(1)}, bf16[24,1024]{1,0:T(8,128)(2,1)S(1)}, u32[]{:S(2)}, u32[]{:S(2)}) collective-permute-start(bf16[24,1024]{1,0:T(8,128)(2,1)S(1)} %get-tuple-element.73), channel_id=1, source_target_pairs={{0,160},{32,192},{64,224},{96,0},{128,32},{160,64},{192,96},{224,1... | collective-permute-start | bytes 147464 | tf_op jit(solution)/shard_map/ppermute | solution.py:22
  171.2 6.1 %collective-permute-start.31 = (bf16[24,1024]{1,0:T(8,128)(2,1)S(1)}, bf16[24,1024]{1,0:T(8,128)(2,1)S(1)}, u32[]{:S(2)}, u32[]{:S(2)}) collective-permute-start(bf16[24,1024]{1,0:T(8,128)(2,1)S(1)} %get-tuple-element.74), channel_id=1, source_target_pairs={{0,192},{32,224},{64,0},{96,32},{128,64},{160,96},{192,128},{224,1... | collective-permute-start | bytes 147464 | tf_op jit(solution)/shard_map/ppermute | solution.py:22
  173.2 5.3 %collective-permute-start.32 = (bf16[24,1024]{1,0:T(8,128)(2,1)S(1)}, bf16[24,1024]{1,0:T(8,128)(2,1)S(1)}, u32[]{:S(2)}, u32[]{:S(2)}) collective-permute-start(bf16[24,1024]{1,0:T(8,128)(2,1)S(1)} %get-tuple-element.75), channel_id=1, source_target_pairs={{0,224},{32,0},{64,32},{96,64},{128,96},{160,128},{192,160},{224,1... | collective-permute-start | bytes 147464 | tf_op jit(solution)/shard_map/ppermute | solution.py:22

commit v2 on v1

--- a/solution.py
+++ b/solution.py
@@ -87,55 +87,49 @@
         all_ref[pl.ds(at, rows), :] = ref[...]
 
 
-def acted(tp_index, normed, blocks, gate_act=None, gates=None):
+def acted(tp_index, normed, gate_blocks, up_blocks, gates):
     tokens, width = normed.shape
-    n = len(blocks)
+    n = len(gate_blocks)
     units = 512
     step = tokens // 2
-    last = gate_act is not None
-
-    def body(tp_ref, n_ref, *refs):
-        all_ref, out_ref = refs[-2:]
-        fill(tp_ref, refs[:n], all_ref)
+
+    def body(tp_ref, n_ref, g_ref, *refs):
+        gate_ref, up_ref, out_ref = refs[-3:]
+        fill(tp_ref, refs[:n], gate_ref)
+        fill(tp_ref, refs[n : 2 * n], up_ref)
         low = lax.broadcasted_iota(jnp.int32, (step, 128), 1) < 64
 
         def one(i, _):
             rows = pl.ds(pl.multiple_of(i * step, step), step)
             for at in range(0, units, 256):
-                act = lax.dot_general(
-                    n_ref[rows, :],
-                    all_ref[pl.ds(at, 256), :],
-                    (((1,), (1,)), ((), ())),
-                    preferred_element_type=jnp.float32,
+                gate, up = (
+                    lax.dot_general(
+                        n_ref[rows, :],
+                        ref[pl.ds(at, 256), :],
+                        (((1,), (1,)), ((), ())),
+                        preferred_element_type=jnp.float32,
+                    )
+                    for ref in (gate_ref, up_ref)
                 )
-                if not last:
-                    out_ref[rows, pl.ds(at, 256)] = act
-                    continue
                 for half in range(2):
-                    cols = pl.ds(at + half * 128, 128)
+                    here = slice(half * 128, (half + 1) * 128)
                     e = (at + half * 128) // 64
-                    mix = jnp.where(
-                        low, refs[n + 1][rows, e : e + 1], refs[n + 1][rows, e + 1 : e + 2]
-                    )
-                    up = act[:, half * 128 : (half + 1) * 128]
-                    hidden = jax.nn.silu(refs[n][rows, cols]) * up * mix
-                    out_ref[rows, cols] = hidden.astype(jnp.bfloat16)
+                    mix = jnp.where(low, g_ref[rows, e : e + 1], g_ref[rows, e + 1 : e + 2])
+                    hidden = jax.nn.silu(gate[:, here]) * up[:, here] * mix
+                    out_ref[rows, pl.ds(at + half * 128, 128)] = hidden.astype(jnp.bfloat16)
             return 0
 
         lax.fori_loop(0, 2, one, 0)
 
-    args = [tp_index, normed, *blocks] + ([gate_act, gates] if last else [])
-    return pl.pallas_call(
-        body,
-        out_shape=[
-            jax.ShapeDtypeStruct((units, width), jnp.bfloat16),
-            jax.ShapeDtypeStruct((tokens, units), jnp.bfloat16 if last else jnp.float32),
-        ],
-        in_specs=[SMEM] + [VMEM] * (len(args) - 1),
-        out_specs=[VMEM] * 2,
-        compiler_params=pltpu.CompilerParams(vmem_limit_bytes=24 << 20),
+    return pl.pallas_call(
+        body,
+        out_shape=[jax.ShapeDtypeStruct((units, width), jnp.bfloat16)] * 2
+        + [jax.ShapeDtypeStruct((tokens, units), jnp.bfloat16)],
+        in_specs=[SMEM] + [VMEM] * (2 + 2 * n),
+        out_specs=[VMEM] * 3,
+        compiler_params=pltpu.CompilerParams(vmem_limit_bytes=28 << 20),
         name="acted",
-    )(*args)
+    )(tp_index, normed, gates, *gate_blocks, *up_blocks)
 
 
 def turned(block, widths):
@@ -361,8 +355,7 @@
     )
     expert_gates = jnp.dot(pick.astype(jnp.float32), expert_gates, precision=lax.Precision.HIGHEST)
 
-    gate_all, gate_act = acted(tp_index, normed, gate_pieces)
-    up_all, hidden = acted(tp_index, normed, up_pieces, gate_act, expert_gates)
+    gate_all, up_all, hidden = acted(tp_index, normed, gate_pieces, up_pieces, expert_gates)
     units = up_all.shape[0] // experts
 
     down_parts, summed = [], []

time: 180 us -> 180 us (level)
    ppermute x33, waiting for transfers between devices: 50.1 us -> 51.9 us  [shifted(): return lax.ppermute(array, axis, [(i, (i + by) % n) for i in range(n)])]
    pallas_call x2 -> x1, Pallas kernels: 5.04 us -> 4.13 us  [acted(): pl.pallas_call(body, out_shape=[jax.ShapeDtypeStruct((units, width), jnp....]
  transfers between devices with their start and end apart: 35 -> 35, of which waited for: 18 -> 19; matrix products, arithmetic and copies ran while one was open for 5% -> 5% of each run, Pallas kernels for 8% -> 8%
where the time goes in v2:
time: 180 us; the launch traced here: 179 us
  waiting for transfers between devices  78.9 us (44%)
  starting transfers between devices  69.5 us (39%)
  Pallas kernels  17.4 us (10%)
  matrix products  5.93 us (3%)
  other arithmetic  3.52 us (2%)
  local copies, waits for them, and re-layouts  3.12 us (2%)
    ppermute x33, waiting for transfers between devices, shifted(): return lax.ppermute(array, axis, [(i, (i + by) % n) for i in range(n)])  51.9 us
    ppermute x33, starting transfers between devices, shifted(): return lax.ppermute(array, axis, [(i, (i + by) % n) for i in range(n)])  50.2 us
    all_to_all x2, waiting for transfers between devices, handed(): return lax.all_to_all(columns, FS, split_axis=0, concat_axis=0, tiled=True)  26.9 us
    all_to_all x2, starting transfers between devices, handed(): return lax.all_to_all(columns, FS, split_axis=0, concat_axis=0, tiled=True)  19.3 us
    dot_general x1, matrix products, local(): jnp.dot(pick.astype(jnp.bfloat16), normed, preferred_element_type=jnp.flo...  4.76 us
    pallas_call x1, Pallas kernels, acted(): pl.pallas_call(body, out_shape=[jax.ShapeDtypeStruct((units, width), jnp....  4.13 us
  transfers between devices with their start and end apart: 35, of which 19 were waited for; matrix products, arithmetic and copies ran while one was open for 5% of the time, Pallas kernels for 8%

profile of v2, /device:TPU:1, one launch (start us, length us, event | category | flops | bytes accessed | tf_op | source)
XLA Modules:
  0.0 179.2 jit_solution(8737531796330486541)
XLA Ops:
  0.6 1.2 copy-done.1
  1.9 1.2 copy-done.2
  3.7 1.5 prepare.2
  5.3 2.2 %collective-permute-start = (bf16[16,2,32,128]{3,2,1,0:T(8,128)(2,1)S(1)}, bf16[16,2,32,128]{3,2,1,0:T(8,128)(2,1)S(1)}, u32[]{:S(2)}, u32[]{:S(2)}) collective-permute-start(bf16[16,2,32,128]{3,2,1,0:T(8,128)(2,1)S(1)} %get-tuple-element.40), channel_id=1, source_target_pairs={{0,1},{1,2},{2,3},{3,0},{4,5},{5,6},{6,7},{7,4},{8,9},{9,10},{10,1... | collective-permute-start | bytes 786440 | tf_op jit(solution)/shard_map/ppermute | solution.py:22
  7.5 2.6 %collective-permute-start.1 = (bf16[16,2,32,128]{3,2,1,0:T(8,128)(2,1)S(1)}, bf16[16,2,32,128]{3,2,1,0:T(8,128)(2,1)S(1)}, u32[]{:S(2)}, u32[]{:S(2)}) collective-permute-start(bf16[16,2,32,128]{3,2,1,0:T(8,128)(2,1)S(1)} %get-tuple-element.41), channel_id=1, source_target_pairs={{0,2},{1,3},{2,0},{3,1},{4,6},{5,7},{6,4},{7,5},{8,10},{9,11},{10,... | collective-permute-start | bytes 786440 | tf_op jit(solution)/shard_map/ppermute | solution.py:22
  10.1 1.1 collective-permute-start.2
  11.1 1.8 %collective-permute-done.refs_1_ = bf16[16,2,32,128]{3,2,1,0:T(8,128)(2,1)S(1)} collective-permute-done((bf16[16,2,32,128]{3,2,1,0:T(8,128)(2,1)S(1)}, bf16[16,2,32,128]{3,2,1,0:T(8,128)(2,1)S(1)}, u32[]{:S(2)}, u32[]{:S(2)}) %collective-permute-start) | collective-permute-done | bytes 262176 | tf_op jit(solution)/shard_map/ppermute | solution.py:22
  13.0 8.4 %collective-permute-done.1.refs_2_ = bf16[16,2,32,128]{3,2,1,0:T(8,128)(2,1)S(1)} collective-permute-done((bf16[16,2,32,128]{3,2,1,0:T(8,128)(2,1)S(1)}, bf16[16,2,32,128]{3,2,1,0:T(8,128)(2,1)S(1)}, u32[]{:S(2)}, u32[]{:S(2)}) %collective-permute-start.1) | collective-permute-done | bytes 262176 | tf_op jit(solution)/shard_map/ppermute | solution.py:22
  21.4 1.0 placed.2
  22.5 13.0 %all-to-all-start = ((bf16[64,2,32,128]{3,2,1,0:T(8,128)(2,1)}), bf16[64,2,32,128]{3,2,1,0:T(8,128)(2,1)S(1)}, u32[]{:S(2)}, u32[]{:S(2)}) async-start(bf16[64,2,32,128]{3,2,1,0:T(8,128)(2,1)} %bitcast.5), calls=%async_computation | async-start | bytes 2097152 | tf_op jit(solution)/shard_map/all_to_all | solution.py:319
  35.5 1.3 prepare.3
  36.8 2.4 %collective-permute-start.10 = (bf16[16,1,32,128]{3,2,1,0:T(8,128)(2,1)S(1)}, bf16[16,1,32,128]{3,2,1,0:T(8,128)(2,1)S(1)}, u32[]{:S(2)}, u32[]{:S(2)}) collective-permute-start(bf16[16,1,32,128]{3,2,1,0:T(8,128)(2,1)S(1)} %get-tuple-element.50), channel_id=1, source_target_pairs={{0,2},{1,3},{2,0},{3,1},{4,6},{5,7},{6,4},{7,5},{8,10},{9,11},{10,... | collective-permute-start | bytes 393224 | tf_op jit(solution)/shard_map/ppermute | solution.py:22
  39.2 1.1 collective-permute-start.11
  40.7 2.3 %collective-permute-done.10.refs_2_ = bf16[16,1,32,128]{3,2,1,0:T(8,128)(2,1)S(1)} collective-permute-done((bf16[16,1,32,128]{3,2,1,0:T(8,128)(2,1)S(1)}, bf16[16,1,32,128]{3,2,1,0:T(8,128)(2,1)S(1)}, u32[]{:S(2)}, u32[]{:S(2)}) %collective-permute-start.10) | collective-permute-done | bytes 131104 | tf_op jit(solution)/shard_map/ppermute | solution.py:22
  43.0 2.3 %collective-permute-done.11.refs_3_ = bf16[16,1,32,128]{3,2,1,0:T(8,128)(2,1)S(1)} collective-permute-done((bf16[16,1,32,128]{3,2,1,0:T(8,128)(2,1)S(1)}, bf16[16,1,32,128]{3,2,1,0:T(8,128)(2,1)S(1)}, u32[]{:S(2)}, u32[]{:S(2)}) %collective-permute-start.11) | collective-permute-done | bytes 131104 | tf_op jit(solution)/shard_map/ppermute | solution.py:22
  45.3 0.9 collective-permute-done.9.refs_1_
  46.2 0.8 placed.3
  47.0 16.7 %all-to-all-done.x_ref = bf16[64,2,32,128]{3,2,1,0:T(8,128)(2,1)S(1)} async-done(((bf16[64,2,32,128]{3,2,1,0:T(8,128)(2,1)}), bf16[64,2,32,128]{3,2,1,0:T(8,128)(2,1)S(1)}, u32[]{:S(2)}, u32[]{:S(2)}) %all-to-all-start) | async-done | bytes 1048608 | tf_op jit(solution)/shard_map/all_to_all | solution.py:319
  63.7 6.3 %all-to-all-start.1 = ((bf16[64,1,32,128]{3,2,1,0:T(8,128)(2,1)}), bf16[64,1,32,128]{3,2,1,0:T(8,128)(2,1)S(1)}, u32[]{:S(2)}, u32[]{:S(2)}) async-start(bf16[64,1,32,128]{3,2,1,0:T(8,128)(2,1)} %bitcast.10), calls=%async_computation.1 | async-start | bytes 1048576 | tf_op jit(solution)/shard_map/all_to_all | solution.py:319
  69.9 2.5 %convert_reduce_fusion = f32[768]{0:T(1024)S(1)} fusion(bf16[768,1,2048]{2,0,1:T(8,128)(2,1)} %param.7), kind=kLoop, calls=%fused_computation | loop fusion | flops 3144960 | bytes 3148800 | tf_op jit(solution)/shard_map/reduce_sum | solution.py:341
  72.5 1.1 turned.2
  73.6 1.0 collective-permute-start.3
  74.7 1.7 collective-permute-start.7
  76.4 1.0 fusion.3
  77.3 10.3 %all-to-all-done.1.x_ref = bf16[64,1,32,128]{3,2,1,0:T(8,128)(2,1)S(1)} async-done(((bf16[64,1,32,128]{3,2,1,0:T(8,128)(2,1)}), bf16[64,1,32,128]{3,2,1,0:T(8,128)(2,1)S(1)}, u32[]{:S(2)}, u32[]{:S(2)}) %all-to-all-start.1) | async-done | bytes 524320 | tf_op jit(solution)/shard_map/all_to_all | solution.py:319
  88.2 1.0 collective-permute-start.15
  89.3 1.7 collective-permute-start.4
  91.0 0.8 collective-permute-start.5
  91.7 2.0 %collective-permute-start.8 = (bf16[128,2048]{1,0:T(8,128)(2,1)S(1)}, bf16[128,2048]{1,0:T(8,128)(2,1)S(1)}, u32[]{:S(2)}, u32[]{:S(2)}) collective-permute-start(bf16[128,2048]{1,0:T(8,128)(2,1)S(1)} %collective-permute-done.7.refs_6_), channel_id=1, source_target_pairs={{0,3},{1,0},{2,1},{3,2},{4,7},{5,4},{6,5},{7,6},{8,11},{9,8},{10,9... | collective-permute-start | bytes 1572872 | tf_op jit(solution)/shard_map/ppermute | solution.py:22
  93.7 4.8 %convolution_convert_fusion.n_ref = bf16[768,2048]{1,0:T(8,128)(2,1)S(1)} fusion(bf16[768,1,2048]{2,0,1:T(8,128)(2,1)} %param.7, f32[768]{0:T(1024)S(1)} %add_rsqrt_fusion, f32[768]{0:T(1024)S(1)} %broadcast_multiply_fusion, s32[768]{0:T(1024)S(1)} %fusion.26), kind=kOutput, calls=%fused_computation.7 | convolution fusion | flops 2424373248 | bytes 6300672 | tf_op jit(solution)/shard_map/dot_general | solution.py:345
  98.5 1.5 collective-permute-start.16
  100.0 2.1 %collective-permute-done.4.refs_2_ = bf16[128,2048]{1,0:T(8,128)(2,1)S(1)} collective-permute-done((bf16[128,2048]{1,0:T(8,128)(2,1)S(1)}, bf16[128,2048]{1,0:T(8,128)(2,1)S(1)}, u32[]{:S(2)}, u32[]{:S(2)}) %collective-permute-start.4) | collective-permute-done | bytes 524320 | tf_op jit(solution)/shard_map/ppermute | solution.py:22
  102.1 2.1 %collective-permute-start.17 = (bf16[128,1024]{1,0:T(8,128)(2,1)S(1)}, bf16[128,1024]{1,0:T(8,128)(2,1)S(1)}, u32[]{:S(2)}, u32[]{:S(2)}) collective-permute-start(bf16[128,1024]{1,0:T(8,128)(2,1)S(1)} %get-tuple-element.54.refs_0_), channel_id=1, source_target_pairs={{0,2},{1,3},{2,0},{3,1},{4,6},{5,7},{6,4},{7,5},{8,10},{9,11},{10,... | collective-permute-start | bytes 786440 | tf_op jit(solution)/shard_map/ppermute | solution.py:22
  104.2 4.0 %collective-permute-done.6.refs_5_ = bf16[128,2048]{1,0:T(8,128)(2,1)S(1)} collective-permute-done((bf16[128,2048]{1,0:T(8,128)(2,1)S(1)}, bf16[128,2048]{1,0:T(8,128)(2,1)S(1)}, u32[]{:S(2)}, u32[]{:S(2)}) %collective-permute-start.6) | collective-permute-done | bytes 524320 | tf_op jit(solution)/shard_map/ppermute | solution.py:22
  108.2 11.2 %collective-permute-done.5.refs_3_ = bf16[128,2048]{1,0:T(8,128)(2,1)S(1)} collective-permute-done((bf16[128,2048]{1,0:T(8,128)(2,1)S(1)}, bf16[128,2048]{1,0:T(8,128)(2,1)S(1)}, u32[]{:S(2)}, u32[]{:S(2)}) %collective-permute-start.5) | collective-permute-done | bytes 524320 | tf_op jit(solution)/shard_map/ppermute | solution.py:22
  120.1 0.9 collective-permute-start.14
  121.0 1.2 fusion.8.g_ref
  122.2 4.1 %acted.1 = (bf16[512,2048]{1,0:T(8,128)(2,1)}, bf16[512,2048]{1,0:T(8,128)(2,1)}, bf16[768,512]{1,0:T(8,128)(2,1)S(1)}) custom-call(s32[1]{0:T(128)} %bitcast.tp_ref, bf16[768,2048]{1,0:T(8,128)(2,1)S(1)} %convolution_convert_fusion.n_ref, f32[768,8]{1,0:T(8,128)S(1)} %fusion.8.g_ref, bf16[128,2048]{1,0:T(8,128)(2,1)S(1)} %get-tuple-element.43.refs_0_, ...), custom_call_target="tpu_custom_call" | custom-call | tf_op jit(solution)/shard_map/acted/pallas_call | solution.py:124
  126.3 1.2 mixed_away.3
  127.5 7.4 %collective-permute-start.22 = (bf16[384,1024]{1,0:T(8,128)(2,1)S(1)}, bf16[384,1024]{1,0:T(8,128)(2,1)S(1)}, u32[]{:S(2)}, u32[]{:S(2)}) collective-permute-start(bf16[384,1024]{1,0:T(8,128)(2,1)S(1)} %get-tuple-element.61), channel_id=1, source_target_pairs={{0,4},{4,0},{1,5},{5,1},{2,6},{6,2},{3,7},{7,3},{8,12},{12,8},{9,1... | collective-permute-start | bytes 2359304 | tf_op jit(solution)/shard_map/ppermute | solution.py:22
  134.9 1.8 %collective-permute-done.14.refs_3_ = bf16[128,1024]{1,0:T(8,128)(2,1)S(1)} collective-permute-done((bf16[128,1024]{1,0:T(8,128)(2,1)S(1)}, bf16[128,1024]{1,0:T(8,128)(2,1)S(1)}, u32[]{:S(2)}, u32[]{:S(2)}) %collective-permute-start.14) | collective-permute-done | bytes 262176 | tf_op jit(solution)/shard_map/ppermute | solution.py:22
  136.7 1.2 mixed_away.2
  137.9 1.6 collective-permute-start.18
  139.5 1.1 mixed_here.3
  140.6 1.2 collective-permute-start.23
  141.7 1.2 collective-permute-start.24
  142.9 1.6 collective-permute-start.25
  144.5 1.1 mixed_here.2
  145.7 1.6 collective-permute-start.20
  147.4 1.4 collective-permute-done.23.refs_5_
  149.0 3.2 %collective-permute-done.24.refs_6_ = bf16[96,1024]{1,0:T(8,128)(2,1)S(1)} collective-permute-done((bf16[96,1024]{1,0:T(8,128)(2,1)S(1)}, bf16[96,1024]{1,0:T(8,128)(2,1)S(1)}, u32[]{:S(2)}, u32[]{:S(2)}) %collective-permute-start.24) | collective-permute-done | bytes 196640 | tf_op jit(solution)/shard_map/ppermute | solution.py:22
  152.1 0.7 collective-permute-done.25.refs_7_
  152.9 4.5 %collective-permute-done.19.refs_1_ = bf16[96,1024]{1,0:T(8,128)(2,1)S(1)} collective-permute-done((bf16[96,1024]{1,0:T(8,128)(2,1)S(1)}, bf16[96,1024]{1,0:T(8,128)(2,1)S(1)}, u32[]{:S(2)}, u32[]{:S(2)}) %collective-permute-start.19) | collective-permute-done | bytes 196640 | tf_op jit(solution)/shard_map/ppermute | solution.py:22
  157.4 3.2 %collective-permute-done.20.refs_2_ = bf16[96,1024]{1,0:T(8,128)(2,1)S(1)} collective-permute-done((bf16[96,1024]{1,0:T(8,128)(2,1)S(1)}, bf16[96,1024]{1,0:T(8,128)(2,1)S(1)}, u32[]{:S(2)}, u32[]{:S(2)}) %collective-permute-start.20) | collective-permute-done | bytes 196640 | tf_op jit(solution)/shard_map/ppermute | solution.py:22
  160.6 0.7 collective-permute-done.21.refs_3_
  161.6 0.8 collective-permute-start.26
  162.4 1.0 collective-permute-start.27
  163.4 2.8 %collective-permute-start.28 = (bf16[24,1024]{1,0:T(8,128)(2,1)S(1)}, bf16[24,1024]{1,0:T(8,128)(2,1)S(1)}, u32[]{:S(2)}, u32[]{:S(2)}) collective-permute-start(bf16[24,1024]{1,0:T(8,128)(2,1)S(1)} %get-tuple-element.69), channel_id=1, source_target_pairs={{0,96},{32,128},{64,160},{96,192},{128,224},{160,0},{192,32},{224,... | collective-permute-start | bytes 147464 | tf_op jit(solution)/shard_map/ppermute | solution.py:22
  166.1 1.9 %collective-permute-start.29 = (bf16[24,1024]{1,0:T(8,128)(2,1)S(1)}, bf16[24,1024]{1,0:T(8,128)(2,1)S(1)}, u32[]{:S(2)}, u32[]{:S(2)}) collective-permute-start(bf16[24,1024]{1,0:T(8,128)(2,1)S(1)} %get-tuple-element.70), channel_id=1, source_target_pairs={{0,128},{32,160},{64,192},{96,224},{128,0},{160,32},{192,64},{224,... | collective-permute-start | bytes 147464 | tf_op jit(solution)/shard_map/ppermute | solution.py:22
  168.1 3.1 %collective-permute-start.30 = (bf16[24,1024]{1,0:T(8,128)(2,1)S(1)}, bf16[24,1024]{1,0:T(8,128)(2,1)S(1)}, u32[]{:S(2)}, u32[]{:S(2)}) collective-permute-start(bf16[24,1024]{1,0:T(8,128)(2,1)S(1)} %get-tuple-element.71), channel_id=1, source_target_pairs={{0,160},{32,192},{64,224},{96,0},{128,32},{160,64},{192,96},{224,1... | collective-permute-start | bytes 147464 | tf_op jit(solution)/shard_map/ppermute | solution.py:22
  171.2 2.0 %collective-permute-start.31 = (bf16[24,1024]{1,0:T(8,128)(2,1)S(1)}, bf16[24,1024]{1,0:T(8,128)(2,1)S(1)}, u32[]{:S(2)}, u32[]{:S(2)}) collective-permute-start(bf16[24,1024]{1,0:T(8,128)(2,1)S(1)} %get-tuple-element.72), channel_id=1, source_target_pairs={{0,192},{32,224},{64,0},{96,32},{128,64},{160,96},{192,128},{224,1... | collective-permute-start | bytes 147464 | tf_op jit(solution)/shard_map/ppermute | solution.py:22
  173.8 1.5 side_by_side.1
  175.3 2.0 %collective-permute-done.31.refs_6_ = bf16[24,1024]{1,0:T(8,128)(2,1)S(1)} collective-permute-done((bf16[24,1024]{1,0:T(8,128)(2,1)S(1)}, bf16[24,1024]{1,0:T(8,128)(2,1)S(1)}, u32[]{:S(2)}, u32[]{:S(2)}) %collective-permute-start.31) | collective-permute-done | bytes 49184 | tf_op jit(solution)/shard_map/ppermute | solution.py:22
  177.3 1.3 collective-permute-done.32.refs_7_
  (44 shorter events, 4.4 us)
Async XLA Ops:
  0.6 1.2 copy-start.1
  1.9 1.2 copy-start.2
  3.1 0.7 copy-start.3
  3.7 31.7 %copy-start = (f32[8,32,1024]{2,1,0:T(8,128)S(1)}, f32[8,32,1024]{2,1,0:T(8,128)}, u32[]{:S(2)}) copy-start(f32[8,32,1024]{2,1,0:T(8,128)} %refs_0_.3) | copy-start | bytes 3145732
  3.7 31.8 %copy-start.4 = (f32[32]{0:T(128)S(1)}, f32[32]{0:T(128)}, u32[]{:S(2)}) copy-start(f32[32]{0:T(128)} %param.8) | copy-start | bytes 388
  5.3 7.7 %collective-permute-start = (bf16[16,2,32,128]{3,2,1,0:T(8,128)(2,1)S(1)}, bf16[16,2,32,128]{3,2,1,0:T(8,128)(2,1)S(1)}, u32[]{:S(2)}, u32[]{:S(2)}) collective-permute-start(bf16[16,2,32,128]{3,2,1,0:T(8,128)(2,1)S(1)} %get-tuple-element.40), channel_id=1, source_target_pairs={{0,1},{1,2},{2,3},{3,0},{4,5},{5,6},{6,7},{7,4},{8,9},{9,10},{10,1... | collective-permute-start | bytes 786440 | tf_op jit(solution)/shard_map/ppermute | solution.py:22
  7.5 14.0 %collective-permute-start.1 = (bf16[16,2,32,128]{3,2,1,0:T(8,128)(2,1)S(1)}, bf16[16,2,32,128]{3,2,1,0:T(8,128)(2,1)S(1)}, u32[]{:S(2)}, u32[]{:S(2)}) collective-permute-start(bf16[16,2,32,128]{3,2,1,0:T(8,128)(2,1)S(1)} %get-tuple-element.41), channel_id=1, source_target_pairs={{0,2},{1,3},{2,0},{3,1},{4,6},{5,7},{6,4},{7,5},{8,10},{9,11},{10,... | collective-permute-start | bytes 786440 | tf_op jit(solution)/shard_map/ppermute | solution.py:22
  10.1 11.3 %collective-permute-start.2 = (bf16[16,2,32,128]{3,2,1,0:T(8,128)(2,1)S(1)}, bf16[16,2,32,128]{3,2,1,0:T(8,128)(2,1)S(1)}, u32[]{:S(2)}, u32[]{:S(2)}) collective-permute-start(bf16[16,2,32,128]{3,2,1,0:T(8,128)(2,1)S(1)} %get-tuple-element.42), channel_id=1, source_target_pairs={{0,3},{1,0},{2,1},{3,2},{4,7},{5,4},{6,5},{7,6},{8,11},{9,8},{10,9... | collective-permute-start | bytes 786440 | tf_op jit(solution)/shard_map/ppermute | solution.py:22
  22.5 41.2 %all-to-all-start = ((bf16[64,2,32,128]{3,2,1,0:T(8,128)(2,1)}), bf16[64,2,32,128]{3,2,1,0:T(8,128)(2,1)S(1)}, u32[]{:S(2)}, u32[]{:S(2)}) async-start(bf16[64,2,32,128]{3,2,1,0:T(8,128)(2,1)} %bitcast.5), calls=%async_computation | async-start | bytes 2097152 | tf_op jit(solution)/shard_map/all_to_all | solution.py:319
  36.8 6.2 %collective-permute-start.10 = (bf16[16,1,32,128]{3,2,1,0:T(8,128)(2,1)S(1)}, bf16[16,1,32,128]{3,2,1,0:T(8,128)(2,1)S(1)}, u32[]{:S(2)}, u32[]{:S(2)}) collective-permute-start(bf16[16,1,32,128]{3,2,1,0:T(8,128)(2,1)S(1)} %get-tuple-element.50), channel_id=1, source_target_pairs={{0,2},{1,3},{2,0},{3,1},{4,6},{5,7},{6,4},{7,5},{8,10},{9,11},{10,... | collective-permute-start | bytes 393224 | tf_op jit(solution)/shard_map/ppermute | solution.py:22
  39.2 6.1 %collective-permute-start.11 = (bf16[16,1,32,128]{3,2,1,0:T(8,128)(2,1)S(1)}, bf16[16,1,32,128]{3,2,1,0:T(8,128)(2,1)S(1)}, u32[]{:S(2)}, u32[]{:S(2)}) collective-permute-start(bf16[16,1,32,128]{3,2,1,0:T(8,128)(2,1)S(1)} %get-tuple-element.51), channel_id=1, source_target_pairs={{0,3},{1,0},{2,1},{3,2},{4,7},{5,4},{6,5},{7,6},{8,11},{9,8},{10,9... | collective-permute-start | bytes 393224 | tf_op jit(solution)/shard_map/ppermute | solution.py:22
  40.2 5.9 %collective-permute-start.9 = (bf16[16,1,32,128]{3,2,1,0:T(8,128)(2,1)S(1)}, bf16[16,1,32,128]{3,2,1,0:T(8,128)(2,1)S(1)}, u32[]{:S(2)}, u32[]{:S(2)}) collective-permute-start(bf16[16,1,32,128]{3,2,1,0:T(8,128)(2,1)S(1)} %get-tuple-element.49), channel_id=1, source_target_pairs={{0,1},{1,2},{2,3},{3,0},{4,5},{5,6},{6,7},{7,4},{8,9},{9,10},{10,1... | collective-permute-start | bytes 393224 | tf_op jit(solution)/shard_map/ppermute | solution.py:22
  63.7 24.0 %all-to-all-start.1 = ((bf16[64,1,32,128]{3,2,1,0:T(8,128)(2,1)}), bf16[64,1,32,128]{3,2,1,0:T(8,128)(2,1)S(1)}, u32[]{:S(2)}, u32[]{:S(2)}) async-start(bf16[64,1,32,128]{3,2,1,0:T(8,128)(2,1)} %bitcast.10), calls=%async_computation.1 | async-start | bytes 1048576 | tf_op jit(solution)/shard_map/all_to_all | solution.py:319
  69.9 6.4 %copy-start.5 = (bf16[768,1,2048]{2,0,1:T(8,128)(2,1)S(1)}, bf16[768,1,2048]{2,0,1:T(8,128)(2,1)}, u32[]{:S(2)}) copy-start(bf16[768,1,2048]{2,0,1:T(8,128)(2,1)} %param.7) | copy-start | bytes 9437188
  73.6 17.4 %collective-permute-start.3 = (bf16[128,2048]{1,0:T(8,128)(2,1)S(1)}, bf16[128,2048]{1,0:T(8,128)(2,1)S(1)}, u32[]{:S(2)}, u32[]{:S(2)}) collective-permute-start(bf16[128,2048]{1,0:T(8,128)(2,1)S(1)} %get-tuple-element.43.refs_0_), channel_id=1, source_target_pairs={{0,1},{1,2},{2,3},{3,0},{4,5},{5,6},{6,7},{7,4},{8,9},{9,10},{10,1... | collective-permute-start | bytes 1572872 | tf_op jit(solution)/shard_map/ppermute | solution.py:22
  74.7 17.1 %collective-permute-start.7 = (bf16[128,2048]{1,0:T(8,128)(2,1)S(1)}, bf16[128,2048]{1,0:T(8,128)(2,1)S(1)}, u32[]{:S(2)}, u32[]{:S(2)}) collective-permute-start(bf16[128,2048]{1,0:T(8,128)(2,1)S(1)} %get-tuple-element.44.refs_4_), channel_id=1, source_target_pairs={{0,3},{1,0},{2,1},{3,2},{4,7},{5,4},{6,5},{7,6},{8,11},{9,8},{10,9... | collective-permute-start | bytes 1572872 | tf_op jit(solution)/shard_map/ppermute | solution.py:22
  88.2 16.0 %copy-start.6 = (f32[768,1,2]{0,2,1:T(2,128)S(1)}, f32[768,1,2]{0,2,1:T(2,128)}, u32[]{:S(2)}) copy-start(f32[768,1,2]{0,2,1:T(2,128)} %param.13) | copy-start | bytes 18436
  88.2 16.0 %copy-start.7 = (s32[768,1,2]{0,2,1:T(2,128)S(1)}, s32[768,1,2]{0,2,1:T(2,128)}, u32[]{:S(2)}) copy-start(s32[768,1,2]{0,2,1:T(2,128)} %param.12) | copy-start | bytes 18436
  88.2 10.3 %collective-permute-start.15 = (bf16[128,1024]{1,0:T(8,128)(2,1)S(1)}, bf16[128,1024]{1,0:T(8,128)(2,1)S(1)}, u32[]{:S(2)}, u32[]{:S(2)}) collective-permute-start(bf16[128,1024]{1,0:T(8,128)(2,1)S(1)} %get-tuple-element.54.refs_0_), channel_id=1, source_target_pairs={{0,1},{1,2},{2,3},{3,0},{4,5},{5,6},{6,7},{7,4},{8,9},{9,10},{10,1... | collective-permute-start | bytes 786440 | tf_op jit(solution)/shard_map/ppermute | solution.py:22
  89.3 12.8 %collective-permute-start.4 = (bf16[128,2048]{1,0:T(8,128)(2,1)S(1)}, bf16[128,2048]{1,0:T(8,128)(2,1)S(1)}, u32[]{:S(2)}, u32[]{:S(2)}) collective-permute-start(bf16[128,2048]{1,0:T(8,128)(2,1)S(1)} %get-tuple-element.43.refs_0_), channel_id=1, source_target_pairs={{0,3},{1,0},{2,1},{3,2},{4,7},{5,4},{6,5},{7,6},{8,11},{9,8},{10,9... | collective-permute-start | bytes 1572872 | tf_op jit(solution)/shard_map/ppermute | solution.py:22
  91.0 17.2 %collective-permute-start.6 = (bf16[128,2048]{1,0:T(8,128)(2,1)S(1)}, bf16[128,2048]{1,0:T(8,128)(2,1)S(1)}, u32[]{:S(2)}, u32[]{:S(2)}) collective-permute-start(bf16[128,2048]{1,0:T(8,128)(2,1)S(1)} %get-tuple-element.44.refs_4_), channel_id=1, source_target_pairs={{0,1},{1,2},{2,3},{3,0},{4,5},{5,6},{6,7},{7,4},{8,9},{9,10},{10,1... | collective-permute-start | bytes 1572872 | tf_op jit(solution)/shard_map/ppermute | solution.py:22
  91.0 28.5 %collective-permute-start.5 = (bf16[128,2048]{1,0:T(8,128)(2,1)S(1)}, bf16[128,2048]{1,0:T(8,128)(2,1)S(1)}, u32[]{:S(2)}, u32[]{:S(2)}) collective-permute-start(bf16[128,2048]{1,0:T(8,128)(2,1)S(1)} %collective-permute-done.3.refs_1_), channel_id=1, source_target_pairs={{0,1},{1,2},{2,3},{3,0},{4,5},{5,6},{6,7},{7,4},{8,9},{9,10},{10,1... | collective-permute-start | bytes 1572872 | tf_op jit(solution)/shard_map/ppermute | solution.py:22
  91.7 28.4 %collective-permute-start.8 = (bf16[128,2048]{1,0:T(8,128)(2,1)S(1)}, bf16[128,2048]{1,0:T(8,128)(2,1)S(1)}, u32[]{:S(2)}, u32[]{:S(2)}) collective-permute-start(bf16[128,2048]{1,0:T(8,128)(2,1)S(1)} %collective-permute-done.7.refs_6_), channel_id=1, source_target_pairs={{0,3},{1,0},{2,1},{3,2},{4,7},{5,4},{6,5},{7,6},{8,11},{9,8},{10,9... | collective-permute-start | bytes 1572872 | tf_op jit(solution)/shard_map/ppermute | solution.py:22
  98.5 27.8 %collective-permute-start.16 = (bf16[128,1024]{1,0:T(8,128)(2,1)S(1)}, bf16[128,1024]{1,0:T(8,128)(2,1)S(1)}, u32[]{:S(2)}, u32[]{:S(2)}) collective-permute-start(bf16[128,1024]{1,0:T(8,128)(2,1)S(1)} %get-tuple-element.54.refs_0_), channel_id=1, source_target_pairs={{0,3},{1,0},{2,1},{3,2},{4,7},{5,4},{6,5},{7,6},{8,11},{9,8},{10,9... | collective-permute-start | bytes 786440 | tf_op jit(solution)/shard_map/ppermute | solution.py:22
  102.1 24.2 %collective-permute-start.17 = (bf16[128,1024]{1,0:T(8,128)(2,1)S(1)}, bf16[128,1024]{1,0:T(8,128)(2,1)S(1)}, u32[]{:S(2)}, u32[]{:S(2)}) collective-permute-start(bf16[128,1024]{1,0:T(8,128)(2,1)S(1)} %get-tuple-element.54.refs_0_), channel_id=1, source_target_pairs={{0,2},{1,3},{2,0},{3,1},{4,6},{5,7},{6,4},{7,5},{8,10},{9,11},{10,... | collective-permute-start | bytes 786440 | tf_op jit(solution)/shard_map/ppermute | solution.py:22
  108.2 26.7 %collective-permute-start.12 = (bf16[128,1024]{1,0:T(8,128)(2,1)S(1)}, bf16[128,1024]{1,0:T(8,128)(2,1)S(1)}, u32[]{:S(2)}, u32[]{:S(2)}) collective-permute-start(bf16[128,1024]{1,0:T(8,128)(2,1)S(1)} %get-tuple-element.52.refs_0_), channel_id=1, source_target_pairs={{0,1},{1,2},{2,3},{3,0},{4,5},{5,6},{6,7},{7,4},{8,9},{9,10},{10,1... | collective-permute-start | bytes 786440 | tf_op jit(solution)/shard_map/ppermute | solution.py:22
  119.4 15.5 %collective-permute-start.13 = (bf16[128,1024]{1,0:T(8,128)(2,1)S(1)}, bf16[128,1024]{1,0:T(8,128)(2,1)S(1)}, u32[]{:S(2)}, u32[]{:S(2)}) collective-permute-start(bf16[128,1024]{1,0:T(8,128)(2,1)S(1)} %get-tuple-element.52.refs_0_), channel_id=1, source_target_pairs={{0,3},{1,0},{2,1},{3,2},{4,7},{5,4},{6,5},{7,6},{8,11},{9,8},{10,9... | collective-permute-start | bytes 786440 | tf_op jit(solution)/shard_map/ppermute | solution.py:22
  120.1 16.6 %collective-permute-start.14 = (bf16[128,1024]{1,0:T(8,128)(2,1)S(1)}, bf16[128,1024]{1,0:T(8,128)(2,1)S(1)}, u32[]{:S(2)}, u32[]{:S(2)}) collective-permute-start(bf16[128,1024]{1,0:T(8,128)(2,1)S(1)} %get-tuple-element.52.refs_0_), channel_id=1, source_target_pairs={{0,2},{1,3},{2,0},{3,1},{4,6},{5,7},{6,4},{7,5},{8,10},{9,11},{10,... | collective-permute-start | bytes 786440 | tf_op jit(solution)/shard_map/ppermute | solution.py:22
  127.5 12.0 %collective-permute-start.22 = (bf16[384,1024]{1,0:T(8,128)(2,1)S(1)}, bf16[384,1024]{1,0:T(8,128)(2,1)S(1)}, u32[]{:S(2)}, u32[]{:S(2)}) collective-permute-start(bf16[384,1024]{1,0:T(8,128)(2,1)S(1)} %get-tuple-element.61), channel_id=1, source_target_pairs={{0,4},{4,0},{1,5},{5,1},{2,6},{6,2},{3,7},{7,3},{8,12},{12,8},{9,1... | collective-permute-start | bytes 2359304 | tf_op jit(solution)/shard_map/ppermute | solution.py:22
  137.9 6.6 %collective-permute-start.18 = (bf16[384,1024]{1,0:T(8,128)(2,1)S(1)}, bf16[384,1024]{1,0:T(8,128)(2,1)S(1)}, u32[]{:S(2)}, u32[]{:S(2)}) collective-permute-start(bf16[384,1024]{1,0:T(8,128)(2,1)S(1)} %get-tuple-element.56), channel_id=1, source_target_pairs={{0,4},{4,0},{1,5},{5,1},{2,6},{6,2},{3,7},{7,3},{8,12},{12,8},{9,1... | collective-permute-start | bytes 2359304 | tf_op jit(solution)/shard_map/ppermute | solution.py:22
  140.6 8.1 %collective-permute-start.23 = (bf16[96,1024]{1,0:T(8,128)(2,1)S(1)}, bf16[96,1024]{1,0:T(8,128)(2,1)S(1)}, u32[]{:S(2)}, u32[]{:S(2)}) collective-permute-start(bf16[96,1024]{1,0:T(8,128)(2,1)S(1)} %get-tuple-element.63), channel_id=1, source_target_pairs={{0,8},{8,16},{16,24},{24,0},{1,9},{9,17},{17,25},{25,1},{2,10},{10... | collective-permute-start | bytes 589832 | tf_op jit(solution)/shard_map/ppermute | solution.py:22
  141.7 10.4 %collective-permute-start.24 = (bf16[96,1024]{1,0:T(8,128)(2,1)S(1)}, bf16[96,1024]{1,0:T(8,128)(2,1)S(1)}, u32[]{:S(2)}, u32[]{:S(2)}) collective-permute-start(bf16[96,1024]{1,0:T(8,128)(2,1)S(1)} %get-tuple-element.64), channel_id=1, source_target_pairs={{0,16},{8,24},{16,0},{24,8},{1,17},{9,25},{17,1},{25,9},{2,18},{10... | collective-permute-start | bytes 589832 | tf_op jit(solution)/shard_map/ppermute | solution.py:22
  142.9 9.9 %collective-permute-start.25 = (bf16[96,1024]{1,0:T(8,128)(2,1)S(1)}, bf16[96,1024]{1,0:T(8,128)(2,1)S(1)}, u32[]{:S(2)}, u32[]{:S(2)}) collective-permute-start(bf16[96,1024]{1,0:T(8,128)(2,1)S(1)} %get-tuple-element.65), channel_id=1, source_target_pairs={{0,24},{8,0},{16,8},{24,16},{1,25},{9,1},{17,9},{25,17},{2,26},{10... | collective-permute-start | bytes 589832 | tf_op jit(solution)/shard_map/ppermute | solution.py:22
  145.6 11.7 %collective-permute-start.19 = (bf16[96,1024]{1,0:T(8,128)(2,1)S(1)}, bf16[96,1024]{1,0:T(8,128)(2,1)S(1)}, u32[]{:S(2)}, u32[]{:S(2)}) collective-permute-start(bf16[96,1024]{1,0:T(8,128)(2,1)S(1)} %get-tuple-element.58), channel_id=1, source_target_pairs={{0,8},{8,16},{16,24},{24,0},{1,9},{9,17},{17,25},{25,1},{2,10},{10... | collective-permute-start | bytes 589832 | tf_op jit(solution)/shard_map/ppermute | solution.py:22
  145.7 14.9 %collective-permute-start.20 = (bf16[96,1024]{1,0:T(8,128)(2,1)S(1)}, bf16[96,1024]{1,0:T(8,128)(2,1)S(1)}, u32[]{:S(2)}, u32[]{:S(2)}) collective-permute-start(bf16[96,1024]{1,0:T(8,128)(2,1)S(1)} %get-tuple-element.59), channel_id=1, source_target_pairs={{0,16},{8,24},{16,0},{24,8},{1,17},{9,25},{17,1},{25,9},{2,18},{10... | collective-permute-start | bytes 589832 | tf_op jit(solution)/shard_map/ppermute | solution.py:22
  148.7 12.6 %collective-permute-start.21 = (bf16[96,1024]{1,0:T(8,128)(2,1)S(1)}, bf16[96,1024]{1,0:T(8,128)(2,1)S(1)}, u32[]{:S(2)}, u32[]{:S(2)}) collective-permute-start(bf16[96,1024]{1,0:T(8,128)(2,1)S(1)} %get-tuple-element.60), channel_id=1, source_target_pairs={{0,24},{8,0},{16,8},{24,16},{1,25},{9,1},{17,9},{25,17},{2,26},{10... | collective-permute-start | bytes 589832 | tf_op jit(solution)/shard_map/ppermute | solution.py:22
  161.6 9.6 %collective-permute-start.26 = (bf16[24,1024]{1,0:T(8,128)(2,1)S(1)}, bf16[24,1024]{1,0:T(8,128)(2,1)S(1)}, u32[]{:S(2)}, u32[]{:S(2)}) collective-permute-start(bf16[24,1024]{1,0:T(8,128)(2,1)S(1)} %get-tuple-element.67), channel_id=1, source_target_pairs={{0,32},{32,64},{64,96},{96,128},{128,160},{160,192},{192,224},{224... | collective-permute-start | bytes 147464 | tf_op jit(solution)/shard_map/ppermute | solution.py:22
  162.4 10.8 %collective-permute-start.27 = (bf16[24,1024]{1,0:T(8,128)(2,1)S(1)}, bf16[24,1024]{1,0:T(8,128)(2,1)S(1)}, u32[]{:S(2)}, u32[]{:S(2)}) collective-permute-start(bf16[24,1024]{1,0:T(8,128)(2,1)S(1)} %get-tuple-element.68), channel_id=1, source_target_pairs={{0,64},{32,96},{64,128},{96,160},{128,192},{160,224},{192,0},{224,... | collective-permute-start | bytes 147464 | tf_op jit(solution)/shard_map/ppermute | solution.py:22
  163.4 11.9 %collective-permute-start.28 = (bf16[24,1024]{1,0:T(8,128)(2,1)S(1)}, bf16[24,1024]{1,0:T(8,128)(2,1)S(1)}, u32[]{:S(2)}, u32[]{:S(2)}) collective-permute-start(bf16[24,1024]{1,0:T(8,128)(2,1)S(1)} %get-tuple-element.69), channel_id=1, source_target_pairs={{0,96},{32,128},{64,160},{96,192},{128,224},{160,0},{192,32},{224,... | collective-permute-start | bytes 147464 | tf_op jit(solution)/shard_map/ppermute | solution.py:22
  166.1 9.1 %collective-permute-start.29 = (bf16[24,1024]{1,0:T(8,128)(2,1)S(1)}, bf16[24,1024]{1,0:T(8,128)(2,1)S(1)}, u32[]{:S(2)}, u32[]{:S(2)}) collective-permute-start(bf16[24,1024]{1,0:T(8,128)(2,1)S(1)} %get-tuple-element.70), channel_id=1, source_target_pairs={{0,128},{32,160},{64,192},{96,224},{128,0},{160,32},{192,64},{224,... | collective-permute-start | bytes 147464 | tf_op jit(solution)/shard_map/ppermute | solution.py:22
  168.1 7.2 %collective-permute-start.30 = (bf16[24,1024]{1,0:T(8,128)(2,1)S(1)}, bf16[24,1024]{1,0:T(8,128)(2,1)S(1)}, u32[]{:S(2)}, u32[]{:S(2)}) collective-permute-start(bf16[24,1024]{1,0:T(8,128)(2,1)S(1)} %get-tuple-element.71), channel_id=1, source_target_pairs={{0,160},{32,192},{64,224},{96,0},{128,32},{160,64},{192,96},{224,1... | collective-permute-start | bytes 147464 | tf_op jit(solution)/shard_map/ppermute | solution.py:22
  171.2 6.1 %collective-permute-start.31 = (bf16[24,1024]{1,0:T(8,128)(2,1)S(1)}, bf16[24,1024]{1,0:T(8,128)(2,1)S(1)}, u32[]{:S(2)}, u32[]{:S(2)}) collective-permute-start(bf16[24,1024]{1,0:T(8,128)(2,1)S(1)} %get-tuple-element.72), channel_id=1, source_target_pairs={{0,192},{32,224},{64,0},{96,32},{128,64},{160,96},{192,128},{224,1... | collective-permute-start | bytes 147464 | tf_op jit(solution)/shard_map/ppermute | solution.py:22
  173.2 5.4 %collective-permute-start.32 = (bf16[24,1024]{1,0:T(8,128)(2,1)S(1)}, bf16[24,1024]{1,0:T(8,128)(2,1)S(1)}, u32[]{:S(2)}, u32[]{:S(2)}) collective-permute-start(bf16[24,1024]{1,0:T(8,128)(2,1)S(1)} %get-tuple-element.73), channel_id=1, source_target_pairs={{0,224},{32,0},{64,32},{96,64},{128,96},{160,128},{192,160},{224,1... | collective-permute-start | bytes 147464 | tf_op jit(solution)/shard_map/ppermute | solution.py:22
